TPU v7x, 768 devices: a whole 4x8x12 slice. The times are simulated.
768 devices in a mesh: tp: 96 (over z, y), dp: 8 (over x, core).
Axes of the slice: x: 4, y: 8, z: 12, core: 2. Of those that a mesh axis runs over, the one named last changes fastest.
Arguments:
- tokens: bfloat16 [192, 8448], P('dp', 'tp'), may hold values from -6 to 6
- gains: float32 [2, 8448], replicated, may hold values from 0.1 to 1.9
- w_input: bfloat16 [2, 8448, 12288], P(None, 'dp', 'tp'), may hold values from -0.0625 to 0.0625
- w_gating: bfloat16 [2, 8448, 12288], P(None, 'dp', 'tp'), may hold values from -0.0625 to 0.0625
- w_output: bfloat16 [2, 12288, 8448], P(None, 'tp'), may hold values from -0.5 to 0.5
- decay_rate: float32 [2, 768, 64], P(None, 'tp'), may hold values from 0.05 to 2
- frequency: float32 [2, 768, 64], P(None, 'tp'), may hold values from -3 to 3
- log_step: float32 [2, 768], P(None, 'tp'), may hold values from -2.3 to 0
- in_real: float32 [2, 768, 64, 16], P(None, 'tp'), may hold values from -1 to 1
- in_imag: float32 [2, 768, 64, 16], P(None, 'tp'), may hold values from -1 to 1
- readout_real_matrix: float32 [2, 768, 16, 64], P(None, 'tp'), may hold values from -0.5 to 0.5
- readout_imag_matrix: float32 [2, 768, 16, 64], P(None, 'tp'), may hold values from -0.5 to 0.5
- skip_gain: float32 [2, 12288], P(None, 'tp'), may hold values from -4 to 4
- state_real: float32 [2, 192, 768, 64], P(None, 'dp', 'tp'), may hold values from -6 to 6
- state_imag: float32 [2, 192, 768, 64], P(None, 'dp', 'tp'), may hold values from -6 to 6
Outputs:
- mixed: bfloat16 [192, 8448], P('dp', 'tp')
- next_real: float32 [2, 192, 768, 64], P(None, 'dp', 'tp')
- next_imag: float32 [2, 192, 768, 64], P(None, 'dp', 'tp')
All inputs are finite; a program needn't handle non-finite values.
Results may differ from a plain program's by a relative error of at most 0.008.
Values may be sent and summed in bfloat16 or wider, within the bound.
A program may use at most 64 MiB of HBM per device.

v0:
```python
import jax
import jax.numpy as jnp
from jax import lax
from jax.sharding import Mesh
from jax.sharding import PartitionSpec as P

GS = 16
LAYERS = 2
TP = ("tp_0", "tp_1")


PRECISION_LEVEL = lax.Precision.HIGHEST


def laid_out(pieces, dim):
    dims = list(pieces.shape[1:])
    dims[dim] *= pieces.shape[0]
    return jnp.moveaxis(pieces, 0, dim).reshape(dims)


def gather_in_order(array, axes, turns):
    pieces = array[None]
    for k in turns:
        pieces = lax.all_gather(pieces, axes[k], axis=0, tiled=True)
    held = [lax.axis_size(axes[k]) for k in reversed(turns)]
    pieces = pieces.reshape(*held, *array.shape)
    turned = sorted(range(len(turns)), key=lambda place: turns[len(turns) - 1 - place])
    return pieces.transpose(*turned, *range(len(turns), pieces.ndim)).reshape(-1, *array.shape)


def gather_axes(array, axes, turns, dim):
    return laid_out(gather_in_order(array, axes, turns), dim)


def scatter_axes(array, axes, dim):
    for axis in axes:
        array = lax.psum_scatter(array, axis, scatter_dimension=dim, tiled=True)
    return array


def sent_together(arrays, axis, dim, along):
    widths = [a.shape[along] for a in arrays]
    both = jnp.concatenate(arrays, axis=along)
    result = lax.all_gather(both, axis, axis=dim, tiled=True)
    return tuple(jnp.split(result, [sum(widths[:k]) for k in range(1, len(widths))], axis=along))


def collect(shard):
    return gather_axes(shard, TP, (0, 1), 1)


def spread(partial_value):
    return scatter_axes(partial_value, TP, 1)


def on_device(
    tokens,
    gains,
    w_input,
    w_gating,
    w_output,
    decay_rate,
    frequency,
    log_step,
    in_real,
    in_imag,
    readout_real_matrix,
    readout_imag_matrix,
    skip_gain,
    state_real,
    state_imag,
):
    batch = tokens.shape[0]
    groups = decay_rate.shape[1]
    shard = tokens
    whole = collect(shard)
    outs_re = []
    outs_im = []
    for layer_params in range(LAYERS):
        xf = whole.astype(jnp.float32)
        meansq = jnp.mean(xf * xf, axis=1, keepdims=True)
        inverse = lax.rsqrt(meansq + 1e-06)
        scaled = (xf * gains[layer_params][None, :]).astype(jnp.bfloat16)
        pieces = sent_together((w_input[layer_params], w_gating[layer_params]), "dp", 0, 1)
        drive = jnp.dot(scaled, pieces[0], preferred_element_type=jnp.float32)
        gate = jnp.dot(scaled, pieces[1], preferred_element_type=jnp.float32)
        drive = drive * inverse
        gate = gate * inverse
        step = jnp.exp(log_step[layer_params])[:, None]
        lam_re = -decay_rate[layer_params]
        lam_im = frequency[layer_params]
        magnitude = jnp.exp(lam_re * step)
        angle = lam_im * step
        abar_re = magnitude * jnp.cos(angle)
        abar_im = magnitude * jnp.sin(angle)
        denom = lam_re * lam_re + lam_im * lam_im
        num_re = abar_re - 1.0
        zoh_re = (num_re * lam_re + abar_im * lam_im) / denom
        zoh_im = (abar_im * lam_re - num_re * lam_im) / denom
        bbar_re = (
            zoh_re[..., None] * in_real[layer_params] - zoh_im[..., None] * in_imag[layer_params]
        )
        bbar_im = (
            zoh_re[..., None] * in_imag[layer_params] + zoh_im[..., None] * in_real[layer_params]
        )
        grouped = drive.reshape(batch, groups, GS)
        push_re = jnp.einsum("bgc,gpc->bgp", grouped, bbar_re, precision=PRECISION_LEVEL)
        push_im = jnp.einsum("bgc,gpc->bgp", grouped, bbar_im, precision=PRECISION_LEVEL)
        old_re = state_real[layer_params]
        old_im = state_imag[layer_params]
        updated_real = abar_re[None] * old_re - abar_im[None] * old_im + push_re
        updated_imag = abar_re[None] * old_im + abar_im[None] * old_re + push_im
        readout_output = jnp.einsum(
            "zju,jiu->zji",
            updated_real,
            readout_real_matrix[layer_params],
            precision=PRECISION_LEVEL,
        ) - jnp.einsum(
            "zju,jiu->zji",
            updated_imag,
            readout_imag_matrix[layer_params],
            precision=PRECISION_LEVEL,
        )
        readout_output = (
            readout_output + skip_gain[layer_params].reshape(groups, GS)[None] * grouped
        )
        gated = (
            jax.nn.gelu(readout_output.reshape(batch, groups * GS)) * jax.nn.sigmoid(gate)
        ).astype(jnp.bfloat16)
        partial_value = jnp.dot(gated, w_output[layer_params], preferred_element_type=jnp.float32)
        outs_re.append(updated_real)
        outs_im.append(updated_imag)
        shard = (shard.astype(jnp.float32) + spread(partial_value)).astype(jnp.bfloat16)
        if layer_params + 1 < LAYERS:
            whole = collect(shard)
    return (shard, jnp.stack(outs_re, axis=0), jnp.stack(outs_im, axis=0))


def solution(mesh):
    torus = Mesh(mesh.devices.reshape(12, 8, mesh.shape["dp"]), ("tp_0", "tp_1", "dp"))
    return jax.shard_map(
        on_device,
        mesh=torus,
        in_specs=(
            P("dp", TP),
            P(),
            P(None, "dp", TP),
            P(None, "dp", TP),
            P(None, TP, None),
            P(None, TP, None),
            P(None, TP, None),
            P(None, TP),
            P(None, TP, None, None),
            P(None, TP, None, None),
            P(None, TP, None, None),
            P(None, TP, None, None),
            P(None, TP),
            P(None, "dp", TP, None),
            P(None, "dp", TP, None),
        ),
        out_specs=(P("dp", TP), P(None, "dp", TP, None), P(None, "dp", TP, None)),
        check_vma=False,
    )
```

profile of v0, /device:TPU:1, one launch (start us, length us, event | category | flops | bytes accessed | tf_op | source)
XLA Modules:
  0.0 438.5 jit_solution(4790599269703238316)
XLA Ops:
  7.2 1.3 slice_bitcast_fusion.2
  8.5 0.9 pad_maximum_fusion
  9.5 28.0 %all-gather = bf16[288,88]{1,0:T(8,128)(2,1)S(1)} all-gather(bf16[24,88]{1,0:T(8,128)(2,1)S(1)} %copy-done.15), channel_id=2, replica_groups=mesh['tp_0'=12,'tp_1'=8,'dp'=8] {'tp_0'}, dimensions={0}, use_global_device_ids=true | all-gather | bytes 54912 | tf_op jit(solution)/shard_map/all_gather | solution.py:24
  37.4 23.5 %all_gather.19 = bf16[96,24,88]{2,1,0:T(8,128)(2,1)S(1)} all-gather(bf16[12,24,88]{2,1,0:T(8,128)(2,1)S(1)} %bitcast.297), channel_id=1, replica_groups=mesh['tp_0'=12,'tp_1'=8,'dp'=8] {'tp_1'}, dimensions={0}, use_global_device_ids=true | all-gather | bytes 456192 | tf_op jit(solution)/shard_map/all_gather | solution.py:24
  61.5 0.6 reshape.348
  62.8 0.7 fusion.137
  63.5 0.7 multiply_bitcast_fusion.1
  64.2 1.0 fusion.154
  65.2 2.1 fusion.22
  67.5 0.4 fusion.16
  67.9 0.4 fusion.17
  68.9 5.6 %convolution_bitcast_fusion.1 = f32[8448,24]{1,0:T(8,128)} fusion(bf16[2,128,8448]{2,1,0:T(8,128)(2,1)} %param.19, bf16[8448,256]{1,0:T(8,128)(2,1)} %all-gather.5.cloned.1.call-done, f32[24,8448]{1,0:T(8,128)S(1)} %reshape.348, f32[8448]{0:T(1024)S(1)} %get-tuple-element.16, f32[24,128]{1,0:T(8,128)S(1)} %copy.84, f32[24]{0:T(128)S(1)} %add_rsqrt_fusion.1), kind=kOutput, calls=%fused_computation.1 | convolution fusion | flops 104257536 | bytes 5993568
  74.5 65.2 %reduce-scatter.9.cloned.1.call-done = f32[704,24]{1,0:T(8,128)} async-done(((f32[8448,24]{1,0:T(8,128)}), f32[704,24]{1,0:T(8,128)}) %reduce-scatter.9.cloned.1.call-update) | async-done | bytes 67600
  139.7 1.8 copy.87
  141.6 0.9 pad_maximum_fusion.1
  142.6 1.3 dynamic-slice
  144.6 78.3 %all-reduce.5.cloned.1.call-done = f32[24,704]{1,0:T(8,128)} async-done(((f32[24,704]{1,0:T(8,128)}), f32[24,704]{1,0:T(8,128)}) %all-reduce.5.cloned.1.call-update) | async-done | bytes 67600
  222.9 0.8 fusion.125
  223.7 19.3 %all-gather.1 = bf16[288,88]{1,0:T(8,128)(2,1)S(1)} all-gather(bf16[24,88]{1,0:T(8,128)(2,1)S(1)} %fusion.125), channel_id=3, replica_groups=mesh['tp_0'=12,'tp_1'=8,'dp'=8] {'tp_0'}, dimensions={0}, use_global_device_ids=true | all-gather | bytes 54912 | tf_op jit(solution)/shard_map/all_gather | solution.py:24
  243.0 21.0 %all_gather.22 = bf16[96,24,88]{2,1,0:T(8,128)(2,1)S(1)} all-gather(bf16[12,24,88]{2,1,0:T(8,128)(2,1)S(1)} %bitcast.298), channel_id=1, replica_groups=mesh['tp_0'=12,'tp_1'=8,'dp'=8] {'tp_1'}, dimensions={0}, use_global_device_ids=true | all-gather | bytes 456192 | tf_op jit(solution)/shard_map/all_gather | solution.py:24
  264.5 0.6 reshape.349
  265.5 4.9 %all-gather.7.cloned.1.call-done = bf16[8448,256]{1,0:T(8,128)(2,1)} async-done(((bf16[1056,256]{1,0:T(8,128)(2,1)}), bf16[8448,256]{1,0:T(8,128)(2,1)}) %all-gather.7.cloned.1.call-update) | async-done | bytes 4325392 | tf_op jit(solution)/shard_map/all_gather | solution.py:44
  270.3 2.1 fusion.43
  272.6 0.4 fusion.14
  273.0 0.4 fusion.15
  274.0 5.6 %convolution_bitcast_fusion = f32[8448,24]{1,0:T(8,128)} fusion(bf16[2,128,8448]{2,1,0:T(8,128)(2,1)} %param.19, bf16[8448,256]{1,0:T(8,128)(2,1)} %all-gather.7.cloned.1.call-done, f32[24,8448]{1,0:T(8,128)S(1)} %reshape.349, f32[8448]{0:T(1024)S(1)} %get-tuple-element.15, f32[24,128]{1,0:T(8,128)S(1)} %copy.85, f32[24]{0:T(128)S(1)} %add_rsqrt_fusion), kind=kOutput, calls=%fused_computation | convolution fusion | flops 104257536 | bytes 5993568
  279.7 0.7 copy.83
  280.4 66.9 %reduce-scatter.11.cloned.1.call-done = f32[704,24]{1,0:T(8,128)} async-done(((f32[8448,24]{1,0:T(8,128)}), f32[704,24]{1,0:T(8,128)}) %reduce-scatter.11.cloned.1.call-update) | async-done | bytes 67600
  347.3 1.8 copy.91
  349.1 0.7 copy.82
  349.8 80.4 %all-reduce.7.cloned.1.call-done = f32[24,704]{1,0:T(8,128)} async-done(((f32[24,704]{1,0:T(8,128)}), f32[24,704]{1,0:T(8,128)}) %all-reduce.7.cloned.1.call-update) | async-done | bytes 67600
  430.2 1.4 fusion.124
  (76 shorter events, 3.7 us)
Async XLA Ops:
  7.2 2.3 copy-start.15
  7.2 58.0 %all-gather.5.cloned.1.call-start = ((), (), s32[]{:S(2)}) async-start(), calls=%async_computation.2 | async-start | bytes 4866048 | tf_op jit(solution)/shard_map/all_gather | solution.py:44
  9.4 130.3 %reduce-scatter.9.cloned.1.call-start = ((), (), s32[]{:S(2)}) async-start(), calls=%async_computation.4 | async-start | bytes 4685824
  61.2 1.0 copy-start.17
  61.2 1.1 copy-start.9
  61.2 1.6 copy-start.18
  61.2 1.6 copy-start.13
  61.2 1.6 copy-start.14
  61.2 3.0 copy-start.4
  62.4 5.1 %copy-start = (f32[2,8,64,16]{2,3,1,0:T(8,128)S(1)}, f32[2,8,64,16]{2,3,1,0:T(8,128)}, u32[]{:S(2)}) copy-start(f32[2,8,64,16]{2,3,1,0:T(8,128)} %param.24) | copy-start | bytes 196612
  62.4 5.1 %copy-start.2 = (f32[2,8,64,16]{2,3,1,0:T(8,128)S(1)}, f32[2,8,64,16]{2,3,1,0:T(8,128)}, u32[]{:S(2)}) copy-start(f32[2,8,64,16]{2,3,1,0:T(8,128)} %param.23) | copy-start | bytes 196612
  65.2 3.1 copy-start.5
  65.2 3.3 copy-start.7
  74.5 148.4 %copy-start.16 = (bf16[24,88]{1,0:T(8,128)(2,1)S(1)}, bf16[24,88]{1,0:T(8,128)(2,1)}, u32[]{:S(2)}) copy-start(bf16[24,88]{1,0:T(8,128)(2,1)} %param.15) | copy-start | bytes 12676
  74.5 148.4 %all-reduce.5.cloned.1.call-start = ((), (), s32[]{:S(2)}) async-start(), calls=%async_computation.6 | async-start | bytes 147456
  141.5 128.8 %all-gather.7.cloned.1.call-start = ((), (), s32[]{:S(2)}) async-start(), calls=%async_computation.3 | async-start | bytes 4866048 | tf_op jit(solution)/shard_map/all_gather | solution.py:44
  142.5 204.8 %reduce-scatter.11.cloned.1.call-start = ((), (), s32[]{:S(2)}) async-start(), calls=%async_computation.5 | async-start | bytes 4685824
  265.1 7.5 %copy-start.1 = (f32[2,8,64,16]{2,3,1,0:T(8,128)S(1)}, f32[2,8,64,16]{2,3,1,0:T(8,128)}, u32[]{:S(2)}) copy-start(f32[2,8,64,16]{2,3,1,0:T(8,128)} %param.24) | copy-start | bytes 196612
  265.1 7.5 %copy-start.3 = (f32[2,8,64,16]{2,3,1,0:T(8,128)S(1)}, f32[2,8,64,16]{2,3,1,0:T(8,128)}, u32[]{:S(2)}) copy-start(f32[2,8,64,16]{2,3,1,0:T(8,128)} %param.23) | copy-start | bytes 196612
  265.1 7.5 %copy-start.10 = (f32[8,64]{1,0:T(8,128)S(1)}, f32[8,64]{1,0:T(8,128)}, u32[]{:S(2)}) copy-start(f32[8,64]{1,0:T(8,128)} %get-tuple-element.28) | copy-start | bytes 6148
  265.1 7.5 %copy-start.11 = (f32[8,64]{1,0:T(8,128)S(1)}, f32[8,64]{1,0:T(8,128)}, u32[]{:S(2)}) copy-start(f32[8,64]{1,0:T(8,128)} %get-tuple-element.29) | copy-start | bytes 6148
  265.2 7.5 %copy-start.12 = (f32[8,64]{1,0:T(8,128)S(1)}, f32[8,64]{1,0:T(8,128)}, u32[]{:S(2)}) copy-start(f32[8,64]{1,0:T(8,128)} %get-tuple-element.30) | copy-start | bytes 6148
  265.5 7.9 %copy-start.6 = (f32[2,8,16,64]{3,2,1,0:T(8,128)S(1)}, f32[2,8,16,64]{3,2,1,0:T(8,128)}, u32[]{:S(2)}) copy-start(f32[2,8,16,64]{3,2,1,0:T(8,128)} %param.25) | copy-start | bytes 196612
  270.3 3.3 copy-start.8
  279.6 150.6 %all-reduce.7.cloned.1.call-start = ((), (), s32[]{:S(2)}) async-start(), calls=%async_computation.7 | async-start | bytes 147456
Sparse Core Ops, SparseCore 0:
  10.4 48.5 all-gather.4
  74.6 65.0 reduce-scatter.8
  142.6 80.2 all-reduce.4
  225.2 45.1 all-gather.6
  279.7 67.4 reduce-scatter.10
  349.4 80.7 all-reduce.6
where the time goes:
time: 444 us; the launch traced here: 438 us
  waiting for transfers between devices  296 us (67%)
  blocking collectives  91.8 us (21%)
  matrix products  18 us (4%)
  between operations  15.2 us (3%)
  local copies, waits for them, and re-layouts  11.3 us (3%)
  other arithmetic  6.18 us (1%)
    unnamed x10, waiting for transfers between devices  291 us
    all_gather x4, blocking collectives, gather_in_order(): pieces = lax.all_gather(pieces, axes[k], axis=0, tiled=True)  91.8 us
    unnamed x2, matrix products  11.1 us
  transfers between devices with their start and end apart: 6, of which 5 were waited for; matrix products, arithmetic and copies ran while one was open for 2% of the time, Pallas kernels for 0%

commit v1 on v0

v1 whole, which is shorter than its diff:
```python
import jax
import jax.numpy as jnp
from jax import lax
from jax.experimental import pallas as pl
from jax.experimental.pallas import tpu as pltpu
from jax.sharding import Mesh
from jax.sharding import PartitionSpec as P

MESH = pl.DeviceIdType.MESH
NZ, NY, NX = 12, 8, 4
LAYERS = 2
B = 24
F = 88
D = NZ * NY * F
C = 128
GROUPS, GS, PS = 8, 16, 64
K = NZ * F
KP = 1152
TILES = KP // 128
BF = jnp.bfloat16
F32 = jnp.float32


def far_first(n):
    return sorted(range(1, n), key=lambda h: -min(h, n - h))


def dot(a, b):
    return jnp.dot(a, b, preferred_element_type=F32)


def dot_t(a, b):
    return lax.dot_general(a, b, (((1,), (1,)), ((), ())), preferred_element_type=F32)


def parts(v):
    hi = v.astype(BF)
    return hi, (v - hi.astype(F32)).astype(BF)


def lanes_of(shape):
    return lax.broadcasted_iota(jnp.int32, shape, 1)


def body(
    tokens, gains, w_in, w_gate, w_out, decay, freq, log_step, in_re, in_im, ro_re, ro_im, skip,
    st_re, st_im,
    mixed, next_re, next_im,
    tok_v, gain_v, win_v, wg_v, wout_v, dec_v, frq_v, ls_v, ire_v, iim_v, rre_v, rim_v, skip_v,
    st_v, s_v, b_hi, b_lo, c_hi, c_lo, nxt_v,
    res_v, zbuf, ybuf, part_v, rsend, rrecv, zsend, zrecv, out_v,
    load_sem, wload_sem, store_sem, zs, zr, ys, yr, rys, ryr, rzs, rzr, xs, xr, cs, cr,
):
    z, y = lax.axis_index("z"), lax.axis_index("y")
    x, c = lax.axis_index("x"), lax.axis_index("c")

    def along(ax, h):
        n = {"z": NZ, "y": NY, "x": NX, "c": 2}[ax]
        return {ax: lax.rem({"z": z, "y": y, "x": x, "c": c}[ax] + h, n)}

    small = [
        (tokens, tok_v), (gains, gain_v), (decay, dec_v), (freq, frq_v), (log_step, ls_v),
        (in_re, ire_v), (in_im, iim_v), (ro_re, rre_v), (ro_im, rim_v), (skip, skip_v),
        (st_re, st_v.at[0]), (st_im, st_v.at[1]),
    ]
    loads = [pltpu.make_async_copy(a, b, load_sem.at[i]) for i, (a, b) in enumerate(small)]
    for cp in loads:
        cp.start()

    def wide(xx, cc):
        return 4 * cc, 3 * xx + 2 * cc

    def rows(zz):
        return pl.ds(pl.multiple_of(zz * F, 8), F)

    wloads = []
    for l in range(LAYERS):
        for m, (src, dst) in enumerate(((w_in, win_v), (w_gate, wg_v))):
            j0, za = wide(x, c)
            wloads.append(pltpu.make_async_copy(
                src.at[l, pl.ds(j0, 8)], dst.at[l, :, rows(za)], wload_sem.at[l, m, 0]))
            wloads.append(pltpu.make_async_copy(
                src.at[l, pl.ds(8 - 8 * c, 4)], dst.at[l, pl.ds(4 * c, 4), rows(3 * x + 1)],
                wload_sem.at[l, m, 1]))
    for cp in wloads:
        cp.start()
    oloads = [pltpu.make_async_copy(w_out.at[l], wout_v.at[l], wload_sem.at[l, 2, 0])
              for l in range(LAYERS)]
    for cp in oloads:
        cp.start()

    barrier = pltpu.get_barrier_semaphore()
    greet = [("z", h) for h in far_first(NZ)] + [("y", h) for h in far_first(NY)]
    greet += [("x", 1), ("x", NX - 1), ("c", 1)]
    for ax, h in greet:
        pl.semaphore_signal(barrier, inc=1, device_id=along(ax, h), device_id_type=MESH)

    for cp in loads:
        cp.wait()

    lane128 = lanes_of((B, 128))
    tp = z * NY + y

    def own_gains(l):
        t0 = (tp * F) // 128 - tp // (NZ * NY - 1)
        g2 = gain_v[pl.ds(l, 1), pl.ds(pl.multiple_of(t0 * 128, 128), 256)]
        g2 = jnp.broadcast_to(g2, (8, 256))
        g2 = pltpu.roll(g2, lax.rem(256 - (tp * F - t0 * 128), 256), 1)
        return g2[0:1, 0:128]

    def publish(l, xv):
        scaled = xv * own_gains(l)
        hi, lo = parts(jnp.sum(xv * xv, axis=1, keepdims=True))
        out = jnp.where(lane128 < F, scaled, 0.0)
        out = jnp.where(lane128 == F, hi.astype(F32), out)
        out = jnp.where(lane128 == F + 1, lo.astype(F32), out)
        zbuf[l, z] = out.astype(BF)

    def z_gather(l):
        return [pltpu.make_async_remote_copy(
            src_ref=zbuf.at[l, z], dst_ref=zbuf.at[l, z], send_sem=zs.at[l], recv_sem=zr.at[l],
            device_id=along("z", h), device_id_type=MESH) for h in far_first(NZ)]

    def z_gather_all(l):
        return pltpu.make_async_remote_copy(
            src_ref=zbuf.at[l, pl.ds(0, NZ - 1)], dst_ref=zbuf.at[l, pl.ds(0, NZ - 1)],
            send_sem=zs.at[l], recv_sem=zr.at[l], device_id=along("z", 1), device_id_type=MESH)

    def compact(l):
        tiles = [jnp.zeros((B, 128), F32) for _ in range(TILES)]
        total = jnp.zeros((B, 128), F32)
        for k in range(NZ):
            v = zbuf[l, k].astype(F32)
            total = total + v
            t, s = divmod(k * F, 128)
            r = pltpu.roll(v, s, 1) if s else v
            tiles[t] = jnp.where((lane128 >= s) & (lane128 < s + F), r, tiles[t])
            if s + F > 128:
                tiles[t + 1] = jnp.where(lane128 < s + F - 128, r, tiles[t + 1])
        sq = jnp.sum(jnp.where((lane128 >= F) & (lane128 < F + 2), total, 0.0), axis=1, keepdims=True)
        hi, lo = parts(sq)
        last = tiles[TILES - 1]
        last = jnp.where(lane128 == 96, hi.astype(F32), last)
        tiles[TILES - 1] = jnp.where(lane128 == 97, lo.astype(F32), last)
        for t in range(TILES):
            ybuf[l, y, :, t * 128:(t + 1) * 128] = tiles[t].astype(BF)

    def y_gather(l):
        return [pltpu.make_async_remote_copy(
            src_ref=ybuf.at[l, y], dst_ref=ybuf.at[l, y], send_sem=ys.at[l], recv_sem=yr.at[l],
            device_id=along("y", h), device_id_type=MESH) for h in far_first(NY)]

    def y_gather_all(l):
        return pltpu.make_async_remote_copy(
            src_ref=ybuf.at[l, pl.ds(0, NY - 1)], dst_ref=ybuf.at[l, pl.ds(0, NY - 1)],
            send_sem=ys.at[l], recv_sem=yr.at[l], device_id=along("y", 1), device_id_type=MESH)

    mats = (win_v, wg_v)

    def rows_copies(l, m, owner_x, owner_c, peer, ss, rs):
        w = mats[m]
        _, za = wide(owner_x, owner_c)
        a = w.at[l, :, rows(za)]
        b = w.at[l, pl.ds(4 * owner_c, 4), rows(3 * owner_x + 1)]
        return [pltpu.make_async_remote_copy(src_ref=r, dst_ref=r, send_sem=ss, recv_sem=rs,
                                             device_id=peer, device_id_type=MESH) for r in (a, b)]

    def rows_wait(l, m, ss, rs):
        w = mats[m].at[l, 0, pl.ds(0, K)]
        return pltpu.make_async_remote_copy(src_ref=w, dst_ref=w, send_sem=ss, recv_sem=rs,
                                            device_id=along("c", 1), device_id_type=MESH)

    right, left = along("x", 1), along("x", NX - 1)
    mate = along("c", 1)
    xr_of = lambda h: lax.rem(x + h, NX)

    x_groups = {
        0: (0, 0, right), 1: (1, 0, left), 2: (1, 0, right), 3: (0, 0, left),
        4: (0, NX - 1, right), 5: (1, 1, left),
    }

    def x_start(l, ids):
        for i in ids:
            m, h, peer = x_groups[i]
            for cp in rows_copies(l, m, xr_of(h), c, peer, xs.at[l, i], xr.at[l, i]):
                cp.start()

    def x_wait_recv(l, ids):
        for i in ids:
            rows_wait(l, x_groups[i][0], xs.at[l, i], xr.at[l, i]).wait_recv()

    def c_start(l, ids):
        for i in ids:
            m, h = i % 2, (0, NX - 1, 1, 2)[i // 2]
            for cp in rows_copies(l, m, xr_of(h), c, mate, cs.at[l, i], cr.at[l, i]):
                cp.start()

    def c_wait_recv(l):
        for i in range(8):
            rows_wait(l, i % 2, cs.at[l, i], cr.at[l, i]).wait_recv()

    def state_prep(l):
        step = jnp.broadcast_to(ls_v[pl.ds(l, 1), :], (GROUPS, GROUPS))
        diag = lax.broadcasted_iota(jnp.int32, (GROUPS, GROUPS), 0) == lanes_of((GROUPS, GROUPS))
        step = jnp.exp(jnp.sum(jnp.where(diag, step, 0.0), axis=1, keepdims=True))
        lr, li = -dec_v[l], frq_v[l]
        mag, ang = jnp.exp(lr * step), li * step
        are, aim = mag * jnp.cos(ang), mag * jnp.sin(ang)
        den = lr * lr + li * li
        nre = are - 1.0
        zre, zim = (nre * lr + aim * li) / den, (aim * lr - nre * li) / den
        a1 = jnp.concatenate([are, are], axis=1)
        a2 = jnp.concatenate([-aim, aim], axis=1)
        spread = lambda v: jnp.broadcast_to(v[:, None, :], (GROUPS, GS, PS)).reshape(C, PS)
        zre, zim = spread(zre), spread(zim)
        ire, iim = ire_v[l], iim_v[l]
        bmat = jnp.concatenate([zre * ire - zim * iim, zre * iim + zim * ire], axis=1)
        cmat = jnp.concatenate([rre_v[l], -rim_v[l]], axis=1)
        group = lax.broadcasted_iota(jnp.int32, (C, 128), 0) // GS
        for g in range(GROUPS):
            at = pl.ds(g * 128, 128)
            b_hi[l, :, at], b_lo[l, :, at] = parts(jnp.where(group == g, bmat, 0.0))
            c_hi[l, :, at], c_lo[l, :, at] = parts(jnp.where(group == g, cmat, 0.0))
            h = jnp.concatenate([st_v[0, l, pl.ds(g, B, stride=GROUPS), :],
                                 st_v[1, l, pl.ds(g, B, stride=GROUPS), :]], axis=1)
            s_v[l, :, at] = a1[g:g + 1] * h + a2[g:g + 1] * pltpu.roll(h, PS, 1)

    def mixer(l):
        drive = jnp.zeros((B, C), F32)
        gate = jnp.zeros((B, C), F32)
        sq = jnp.zeros((B, 128), F32)
        for k in range(NY):
            a = ybuf[l, k]
            drive = drive + dot(a[:, :K], win_v[l, k])
            gate = gate + dot(a[:, :K], wg_v[l, k])
            sq = sq + a[:, KP - 128:].astype(F32)
        sq = jnp.sum(jnp.where((lane128 >= 96) & (lane128 < 98), sq, 0.0), axis=1, keepdims=True)
        inverse = lax.rsqrt(sq * (1.0 / D) + 1e-06)
        drive, gate = drive * inverse, gate * inverse
        uh, ul = parts(drive)
        bh, bl = b_hi[l], b_lo[l]
        h = s_v[l] + (dot(uh, bh) + (dot(uh, bl) + dot(ul, bh)))
        hh, hl = parts(h)
        ch, cl = c_hi[l], c_lo[l]
        out = dot_t(hh, ch) + (dot_t(hh, cl) + dot_t(hl, ch))
        out = out + skip_v[pl.ds(l, 1), :] * drive
        s_v[l] = h
        gelu = 0.5 * out * (1.0 + jnp.tanh(0.7978845608028654 * (out + 0.044715 * (out * out * out))))
        return (gelu * (1.0 / (1.0 + jnp.exp(-gate)))).astype(BF)

    def store_states(l):
        for g in range(GROUPS):
            h = s_v[l, :, pl.ds(g * 128, 128)]
            nxt_v[0, l, pl.ds(g, B, stride=GROUPS), :] = h[:, :PS]
            nxt_v[1, l, pl.ds(g, B, stride=GROUPS), :] = pltpu.roll(h, PS, 1)[:, :PS]

    def project(l, gated):
        part_v[...] = dot(gated, wout_v[l])
        for yy in range(NY):
            tiles = [jnp.zeros((B, 128), F32) for _ in range(TILES)]
            for k in range(NZ):
                lo = (k * NY + yy) * F
                done = 0
                while done < F:
                    st, so = divmod(lo + done, 128)
                    tt, to = divmod(k * F + done, 128)
                    n = min(F - done, 128 - so, 128 - to)
                    v = part_v[:, st * 128:(st + 1) * 128]
                    sh = (to - so) % 128
                    v = pltpu.roll(v, sh, 1) if sh else v
                    tiles[tt] = jnp.where((lane128 >= to) & (lane128 < to + n), v, tiles[tt])
                    done += n
            for t in range(TILES):
                rsend[l, yy, :, t * 128:(t + 1) * 128] = tiles[t].astype(BF)

    def y_scatter(l):
        out = []
        for h in far_first(NY):
            to = lax.rem(y + h, NY)
            out.append(pltpu.make_async_remote_copy(
                src_ref=rsend.at[l, to], dst_ref=rrecv.at[l, h - 1], send_sem=rys.at[l],
                recv_sem=ryr.at[l], device_id={"y": to}, device_id_type=MESH))
        return out

    def y_scatter_all(l):
        return pltpu.make_async_remote_copy(
            src_ref=rrecv.at[l], dst_ref=rrecv.at[l], send_sem=rys.at[l], recv_sem=ryr.at[l],
            device_id=along("y", 1), device_id_type=MESH)

    def y_sum(l):
        total = rsend[l, y].astype(F32)
        for h in range(NY - 1):
            total = total + rrecv[l, h].astype(F32)
        tiles = [total[:, t * 128:(t + 1) * 128] for t in range(TILES)]
        for k in range(NZ):
            t, s = divmod(k * F, 128)
            v = pltpu.roll(tiles[t], 128 - s, 1) if s else tiles[t]
            if s + F > 128:
                w = pltpu.roll(tiles[t + 1], 128 - s, 1)
                v = jnp.where(lane128 < 128 - s, v, w)
            zsend[l, k] = v.astype(BF)

    def z_scatter(l):
        out = []
        for h in far_first(NZ):
            to = lax.rem(z + h, NZ)
            out.append(pltpu.make_async_remote_copy(
                src_ref=zsend.at[l, to], dst_ref=zrecv.at[l, h - 1], send_sem=rzs.at[l],
                recv_sem=rzr.at[l], device_id={"z": to}, device_id_type=MESH))
        return out

    def z_scatter_all(l):
        return pltpu.make_async_remote_copy(
            src_ref=zrecv.at[l], dst_ref=zrecv.at[l], send_sem=rzs.at[l], recv_sem=rzr.at[l],
            device_id=along("z", 1), device_id_type=MESH)

    def z_sum(l):
        total = zsend[l, z].astype(F32)
        for h in range(NZ - 1):
            total = total + zrecv[l, h].astype(F32)
        return total

    res_v[...] = jnp.zeros((B, 128), F32)
    res_v[:, :F] = tok_v[...].astype(F32)
    publish(0, res_v[...])
    for cp in wloads + oloads:
        cp.wait()
    pl.semaphore_wait(barrier, len(greet))

    for l in range(LAYERS):
        for cp in z_gather(l):
            cp.start()
        if l == 0:
            x_start(0, (0, 1, 2, 3))
            c_start(0, (0, 1))
            state_prep(0)
        else:
            x_wait_recv(1, (4, 5))
            c_start(1, (6, 7))
        z_gather_all(l).wait_recv()
        compact(l)
        for cp in y_gather(l):
            cp.start()
        if l == 0:
            x_wait_recv(0, (0, 1))
            x_start(0, (4, 5))
            c_start(0, (2, 5))
            state_prep(1)
            x_wait_recv(0, (2, 3))
            c_start(0, (3, 4))
        y_gather_all(l).wait_recv()
        if l == 0:
            x_wait_recv(0, (4, 5))
            c_start(0, (6, 7))
            x_start(1, (0, 1, 2, 3))
            c_start(1, (0, 1))
        c_wait_recv(l)
        gated = mixer(l)
        project(l, gated)
        for cp in y_scatter(l):
            cp.start()
        store_states(l)
        if l == 0:
            x_wait_recv(1, (0, 1))
            x_start(1, (4, 5))
            c_start(1, (2, 5))
        else:
            outs = [pltpu.make_async_copy(nxt_v.at[i], (next_re, next_im)[i], store_sem.at[i])
                    for i in range(2)]
            for cp in outs:
                cp.start()
        y_scatter_all(l).wait_recv()
        y_sum(l)
        for cp in z_scatter(l):
            cp.start()
        if l == 0:
            x_wait_recv(1, (2, 3))
            c_start(1, (3, 4))
        z_scatter_all(l).wait_recv()
        new = jnp.where(lane128 < F, res_v[...] + z_sum(l), 0.0).astype(BF)
        if l + 1 < LAYERS:
            res_v[...] = new.astype(F32)
            publish(l + 1, new.astype(F32))
        else:
            out_v[...] = new[:, :F]
    cp = pltpu.make_async_copy(out_v, mixed, store_sem.at[2])
    cp.start()
    for l in range(LAYERS):
        z_gather_all(l).wait_send()
        y_gather_all(l).wait_send()
        y_scatter_all(l).wait_send()
        z_scatter_all(l).wait_send()
        for i in range(6):
            rows_wait(l, x_groups[i][0], xs.at[l, i], xr.at[l, i]).wait_send()
        for i in range(8):
            rows_wait(l, i % 2, cs.at[l, i], cr.at[l, i]).wait_send()
    for o in outs:
        o.wait()
    cp.wait()


def on_device(tokens, gains, w_in, w_gate, w_out, decay, freq, log_step, in_re, in_im, ro_re, ro_im,
              skip, st_re, st_im):
    blocks = lambda w: w.reshape(LAYERS, NZ, F, C)
    flat = lambda s: s.reshape(LAYERS, B * GROUPS, PS)
    cols = lambda m: m.transpose(0, 1, 3, 2).reshape(LAYERS, C, PS)
    wide = lambda m: m.reshape(LAYERS, C, PS)
    args = (tokens, gains, blocks(w_in), blocks(w_gate), w_out, decay, freq, log_step, cols(in_re),
            cols(in_im), wide(ro_re), wide(ro_im), skip, flat(st_re), flat(st_im))
    any_ = pl.BlockSpec(memory_space=pl.ANY)
    V = pltpu.VMEM
    sem = pltpu.SemaphoreType.DMA
    L = LAYERS
    scratch = [
        V((B, F), BF), V((L, D), F32),
        V((L, NY, K, C), BF), V((L, NY, K, C), BF), V((L, C, D), BF),
        V((L, GROUPS, PS), F32), V((L, GROUPS, PS), F32), V((L, GROUPS), F32),
        V((L, C, PS), F32), V((L, C, PS), F32), V((L, C, PS), F32), V((L, C, PS), F32), V((L, C), F32),
        V((2, L, B * GROUPS, PS), F32), V((L, B, GROUPS * 128), F32),
        V((L, C, GROUPS * 128), BF), V((L, C, GROUPS * 128), BF),
        V((L, C, GROUPS * 128), BF), V((L, C, GROUPS * 128), BF),
        V((2, L, B * GROUPS, PS), F32),
        V((B, 128), F32), V((L, NZ, B, 128), BF), V((L, NY, B, KP), BF), V((B, D), F32),
        V((L, NY, B, KP), BF), V((L, NY - 1, B, KP), BF),
        V((L, NZ, B, 128), BF), V((L, NZ - 1, B, 128), BF), V((B, F), BF),
        sem((12,)), sem((L, 3, 2)), sem((3,)),
        sem((L,)), sem((L,)), sem((L,)), sem((L,)), sem((L,)), sem((L,)), sem((L,)), sem((L,)),
        sem((L, 6)), sem((L, 6)), sem((L, 8)), sem((L, 8)),
    ]
    mixed, nre, nim = pl.pallas_call(
        body,
        name="decode",
        out_shape=(jax.ShapeDtypeStruct((B, F), BF),
                   jax.ShapeDtypeStruct((L, B * GROUPS, PS), F32),
                   jax.ShapeDtypeStruct((L, B * GROUPS, PS), F32)),
        in_specs=[any_] * len(args),
        out_specs=(any_,) * 3,
        scratch_shapes=scratch,
        compiler_params=pltpu.CompilerParams(collective_id=0, has_side_effects=True,
                                             vmem_limit_bytes=56 * 2**20),
    )(*args)
    shape = (L, B, GROUPS, PS)
    return mixed, nre.reshape(shape), nim.reshape(shape)


def solution(mesh):
    torus = Mesh(mesh.devices.reshape(NZ, NY, NX, 2), ("z", "y", "x", "c"))
    tp, dp = ("z", "y"), ("x", "c")
    return jax.shard_map(
        on_device,
        mesh=torus,
        in_specs=(
            P(dp, tp), P(), P(None, dp, tp), P(None, dp, tp), P(None, tp, None), P(None, tp, None),
            P(None, tp, None), P(None, tp), P(None, tp, None, None), P(None, tp, None, None),
            P(None, tp, None, None), P(None, tp, None, None), P(None, tp),
            P(None, dp, tp, None), P(None, dp, tp, None),
        ),
        out_specs=(P(dp, tp), P(None, dp, tp, None), P(None, dp, tp, None)),
        check_vma=False,
    )
```

time: 444 us -> 102 us (0.23); the launches traced: 438 us -> 102 us
  waiting for transfers between devices: 296 us -> 0 us
  Pallas kernels: 0 us -> 96.6 us
  blocking collectives: 91.8 us -> 0 us
  matrix products: 18 us -> 0 us
  between operations: 15.2 us -> 0.65 us
  local copies, waits for them, and re-layouts: 11.3 us -> 4.52 us
  other arithmetic: 6.18 us -> 0 us
    unnamed x10 -> x0, waiting for transfers between devices: 291 us -> none
    pallas_call x0 -> x1, Pallas kernels: none -> 96.6 us  [on_device(): pl.pallas_call(body, name='decode', out_shape=(jax.ShapeDtypeStruct((B, F...]
    all_gather x4 -> x0, blocking collectives: 91.8 us -> none  [gather_in_order(): pieces = lax.all_gather(pieces, axes[k], axis=0, tiled=True)]
    unnamed x2 -> x0, matrix products: 11.1 us -> none
    dot_general x10 -> x0, matrix products: 6.83 us -> none  [the longest x2 4.22 us: on_device(): drive = jnp.dot(scaled, pieces[0], preferred_element_type=jnp.float32)]
    all_gather x2 -> x0, waiting for transfers between devices: 4.89 us -> none  [sent_together(): result = lax.all_gather(both, axis, axis=dim, tiled=True)]
  transfers between devices with their start and end apart: 6 -> 0, of which waited for: 5 -> 0; matrix products, arithmetic and copies ran while one was open for 2% -> 0% of each run, Pallas kernels for 0% -> 0%
where the time goes in v1:
time: 102 us
  Pallas kernels  96.6 us (95%)
  local copies, waits for them, and re-layouts  4.52 us (4%)
    pallas_call x1, Pallas kernels, on_device(): pl.pallas_call(body, name='decode', out_shape=(jax.ShapeDtypeStruct((B, F...  96.6 us
    unnamed x3, local copies, waits for them, and re-layouts  4.52 us

profile of v1, /device:TPU:1, one launch (start us, length us, event | category | flops | bytes accessed | tf_op | source)
XLA Modules:
  0.0 101.8 jit_solution(5304597123955677330)
XLA Ops:
  0.6 96.6 %decode.1 = (bf16[24,88]{1,0:T(8,128)(2,1)}, f32[2,192,64]{2,1,0:T(8,128)}, f32[2,192,64]{2,1,0:T(8,128)}) custom-call(bf16[24,88]{1,0:T(8,128)(2,1)} %tokens.1, f32[2,8448]{1,0:T(2,128)} %gains.1, bf16[2,12,88,128]{3,2,1,0:T(8,128)(2,1)} %bitcast.14, bf16[2,12,88,128]{3,2,1,0:T(8,128)(2,1)} %bitcast.15, bf16[2,128,8448]{2,1,0:T(8,128)(2,1)} %w_out.1, ...), custom_call_target="tpu_custom_call" | custom-call | tf_op jit(solution)/shard_map/decode/pallas_call | solution.py:430
  97.3 1.3 %copy.21 = bf16[24,88]{1,0:T(8,128)(2,1)} copy(bf16[24,88]{1,0:T(8,128)(2,1)} %get-tuple-element.12) | data formatting | bytes 8448
  98.6 1.6 %copy.22 = f32[2,24,8,64]{3,2,1,0:T(8,128)} copy(f32[2,24,8,64]{3,2,1,0:T(8,128)} %bitcast.19) | data formatting | bytes 196608
  100.2 1.6 %copy.23 = f32[2,24,8,64]{3,2,1,0:T(8,128)} copy(f32[2,24,8,64]{3,2,1,0:T(8,128)} %bitcast.18) | data formatting | bytes 196608

commit v2 on v1

v2 whole, which is shorter than its diff:
```python
import jax
import jax.numpy as jnp
from jax import lax
from jax.experimental import pallas as pl
from jax.experimental.pallas import tpu as pltpu
from jax.sharding import Mesh
from jax.sharding import PartitionSpec as P

MESH = pl.DeviceIdType.MESH
NZ, NY, NX = 12, 8, 4
LAYERS = 2
B = 24
F = 88
D = NZ * NY * F
C = 128
GROUPS, GS, PS = 8, 16, 64
K = NZ * F
KP = 1152
TILES = KP // 128
SEMS = 80
BF = jnp.bfloat16
F32 = jnp.float32


def far_first(n):
    return sorted(range(1, n), key=lambda h: -min(h, n - h))


def dot(a, b):
    return jnp.dot(a, b, preferred_element_type=F32)


def dot_t(a, b):
    return lax.dot_general(a, b, (((1,), (1,)), ((), ())), preferred_element_type=F32)


def parts(v):
    hi = v.astype(BF)
    return hi, (v - hi.astype(F32)).astype(BF)


def lanes_of(shape):
    return lax.broadcasted_iota(jnp.int32, shape, 1)


def body(
    tokens, gains, w_in, w_gate, w_out, decay, freq, log_step, in_re, in_im, ro_re, ro_im, skip,
    st_re, st_im,
    mixed, next_re, next_im,
    tok_v, gain_v, win_v, wg_v, stage_v, wout_v, wrow_v, wsend_v, wo_v,
    dec_v, frq_v, ls_v, ire_v, iim_v, rre_v, rim_v, skip_v,
    st_v, s_v, b_hi, b_lo, c_hi, c_lo,
    res_v, zbuf, ybuf, xl_v, part_v, rsend, rrecv, psend, precv, gbuf, zsend, zrecv,
    load_sem, wload_sem, ssem, rsem,
):
    z, y = lax.axis_index("z"), lax.axis_index("y")
    x, c = lax.axis_index("x"), lax.axis_index("c")
    scope = jax.named_scope

    def along(ax, h):
        n = {"z": NZ, "y": NY, "x": NX, "c": 2}[ax]
        return {ax: lax.rem({"z": z, "y": y, "x": x, "c": c}[ax] + h, n)}

    right, left, mate = along("x", 1), along("x", NX - 1), along("c", 1)

    barrier = pltpu.get_barrier_semaphore()
    greet = [("z", h) for h in far_first(NZ)] + [("y", h) for h in far_first(NY)]
    greet += [("x", 1), ("x", NX - 1), ("c", 1)]
    for ax, h in greet:
        pl.semaphore_signal(barrier, inc=1, device_id=along(ax, h), device_id_type=MESH)

    small = [
        (tokens, tok_v), (gains, gain_v), (decay, dec_v), (freq, frq_v), (log_step, ls_v),
        (in_re, ire_v), (in_im, iim_v), (ro_re, rre_v), (ro_im, rim_v), (skip, skip_v),
        (st_re, st_v.at[0]), (st_im, st_v.at[1]),
    ]
    loads = [pltpu.make_async_copy(a, b, load_sem.at[i]) for i, (a, b) in enumerate(small)]
    for cp in loads:
        cp.start()

    def rows(zz):
        return pl.ds(pl.multiple_of(zz * F, 8), F)

    mats = (win_v, wg_v)
    d16 = pl.ds(pl.multiple_of((2 * x + c) * 16, 16), 16)
    za, zb = 3 * x + 2 * c, 3 * x + 1
    has_b = (y // 4) == c

    def load(src, dst, k):
        cp = pltpu.make_async_copy(src, dst, wload_sem.at[k])
        cp.start()
        return cp

    wloads0 = []
    for m, src in enumerate((w_in, w_gate)):
        wloads0.append(load(src.at[0, pl.ds(4 * c, 8)], mats[m].at[0, :, rows(za)], 2 * m))
        wloads0.append(load(src.at[0, pl.ds(8 - 8 * c, 4)],
                            mats[m].at[0, pl.ds(4 * c, 4), rows(zb)], 2 * m + 1))
    oload = load(w_out.at[0], wout_v, 4)
    wloads1 = []
    for m, src in enumerate((w_in, w_gate)):
        wloads1.append(load(src.at[1], stage_v.at[m], 5 + m))
        wloads1.append(load(src.at[1, 4 * c + y], mats[m].at[1, y, rows(za)], 7 + m))
    rload = load(w_out.at[1, d16], wrow_v, 9)

    def own_b(m):
        src = (w_in, w_gate)[m]
        return pltpu.make_async_copy(
            src.at[1, 8 - 8 * c + lax.rem(y, 4)], mats[m].at[1, y, rows(zb)], wload_sem.at[10 + m])

    @pl.when(has_b)
    def _():
        own_b(0).start()
        own_b(1).start()

    names = {}

    def sem_of(key):
        return names.setdefault(key, len(names))

    def remote(src, dst, key, peer):
        k = sem_of(key)
        return pltpu.make_async_remote_copy(src_ref=src, dst_ref=dst, send_sem=ssem.at[k],
                                            recv_sem=rsem.at[k], device_id=peer, device_id_type=MESH)

    unsent = []

    def group(key, copies, size):
        for src, dst, peer in copies:
            remote(src, dst, key, peer).start()
        unsent.append((key, size))

    def arrived(key, size):
        remote(size, size, key, mate).wait_recv()

    with scope("small_loads"):
        for cp in loads:
            cp.wait()

    lane128 = lanes_of((B, 128))
    tp = z * NY + y

    def own_gains(l):
        t0 = (tp * F) // 128 - tp // (NZ * NY - 1)
        g2 = gain_v[pl.ds(l, 1), pl.ds(pl.multiple_of(t0 * 128, 128), 256)]
        g2 = jnp.broadcast_to(g2, (8, 256))
        g2 = pltpu.roll(g2, lax.rem(256 - (tp * F - t0 * 128), 256), 1)
        return g2[0:1, 0:128]

    def publish(l, xv):
        scaled = xv * own_gains(l)
        hi, lo = parts(jnp.sum(xv * xv, axis=1, keepdims=True))
        out = jnp.where(lane128 < F, scaled, 0.0)
        out = jnp.where(lane128 == F, hi.astype(F32), out)
        out = jnp.where(lane128 == F + 1, lo.astype(F32), out)
        zbuf[l, z] = out.astype(BF)

    def gather(key, buf, ax, n, me):
        group(key, [(buf.at[me], buf.at[me], along(ax, h)) for h in far_first(n)],
              buf.at[pl.ds(0, n - 1)])

    def scatter(key, src, dst, ax, n, me):
        copies = []
        for h in far_first(n):
            to = lax.rem(me + h, n)
            copies.append((src.at[to], dst.at[h - 1], {ax: to}))
        group(key, copies, dst)

    def compact(l, write):
        tiles = [jnp.zeros((B, 128), F32) for _ in range(TILES)]
        total = jnp.zeros((B, 128), F32)
        for k in range(NZ):
            v = zbuf[l, k].astype(F32)
            total = total + v
            t, s = divmod(k * F, 128)
            r = pltpu.roll(v, s, 1) if s else v
            tiles[t] = jnp.where((lane128 >= s) & (lane128 < s + F), r, tiles[t])
            if s + F > 128:
                tiles[t + 1] = jnp.where(lane128 < s + F - 128, r, tiles[t + 1])
        sq = jnp.sum(jnp.where((lane128 >= F) & (lane128 < F + 2), total, 0.0), axis=1, keepdims=True)
        hi, lo = parts(sq)
        last = tiles[TILES - 1]
        last = jnp.where(lane128 == 96, hi.astype(F32), last)
        tiles[TILES - 1] = jnp.where(lane128 == 97, lo.astype(F32), last)
        for t in range(TILES):
            write(t, tiles[t].astype(BF))

    def ring0(key, m, owner_x, peer):
        w = mats[m]
        a = w.at[0, :, rows(3 * owner_x + 2 * c)]
        b = w.at[0, pl.ds(4 * c, 4), rows(3 * owner_x + 1)]
        group(key, [(a, a, peer), (b, b, peer)], w.at[0, 0, pl.ds(0, K)])

    def ring0_wait(key):
        arrived(key, win_v.at[0, 0, pl.ds(0, K)])

    def ring1(key, m, owner_x, peer):
        w = mats[m]
        a = w.at[1, :, rows(3 * owner_x + 2 * c)]
        group(key + "a", [(a, a, peer)], a)
        b = w.at[1, :, rows(3 * owner_x + 1)]

        @pl.when(has_b)
        def _():
            remote(b, b, key + "b", peer).start()

        part_sent.append((key + "b", b, has_b))

    part_sent = []
    blocks8 = win_v.at[1, :, pl.ds(0, F)]

    def ring1_wait(key):
        arrived(key + "a", blocks8)

        @pl.when(has_b)
        def _():
            arrived(key + "b", blocks8)

    def mate1_wait(key):
        arrived(key + "a", blocks8)

        @pl.when(jnp.logical_not(has_b))
        def _():
            arrived(key + "b", blocks8)

    def exchange1(m):
        key, w = f"e{m}", mats[m]
        dst = w.at[1, y, rows(za)]
        copies = []
        for h in far_first(NY):
            to = lax.rem(y + h, NY)
            copies.append((stage_v.at[m, 4 * c + to], dst, {"y": to}))
        group(key + "a", copies, w.at[1, pl.ds(0, NY - 1), pl.ds(0, F)])
        dst_b = w.at[1, y, rows(zb)]
        for k in range(4):
            to = 4 * c + k

            @pl.when(to != y)
            def _():
                remote(stage_v.at[m, 8 - 8 * c + k], dst_b, key + "b", {"y": to}).start()

        part_sent.append((key + "b", w.at[1, pl.ds(0, 3), pl.ds(0, F)], has_b))
        part_sent.append((key + "b", w.at[1, pl.ds(0, 4), pl.ds(0, F)], jnp.logical_not(has_b)))

    def exchange1_wait(m):
        key, w = f"e{m}", mats[m]
        arrived(key + "a", w.at[1, pl.ds(0, NY - 1), pl.ds(0, F)])

        @pl.when(has_b)
        def _():
            arrived(key + "b", w.at[1, pl.ds(0, NY - 1), pl.ds(0, F)])

    x_of = lambda h: lax.rem(x + h, NX)
    names_of = ("in", "gate")

    def wo_rows(h, cc):
        return pl.ds(pl.multiple_of((2 * x_of(h) + cc) * 16, 16), 16)

    def relayout_out():
        lane16 = lanes_of((16, 128))
        for yy in range(NY):
            tiles = [jnp.zeros((16, 128), F32) for _ in range(TILES)]
            by_y(lambda st: wrow_v[:, st * 128:(st + 1) * 128].astype(F32), yy, tiles, lane16)
            for t in range(TILES):
                wsend_v[yy, :, t * 128:(t + 1) * 128] = tiles[t].astype(BF)
        wo_v[y, d16] = wsend_v[y]

    def by_y(tile_of, yy, tiles, lane):
        for k in range(NZ):
            lo, done = (k * NY + yy) * F, 0
            while done < F:
                st, so = divmod(lo + done, 128)
                tt, to = divmod(k * F + done, 128)
                n = min(F - done, 128 - so, 128 - to)
                v, sh = tile_of(st), (to - so) % 128
                v = pltpu.roll(v, sh, 1) if sh else v
                tiles[tt] = jnp.where((lane >= to) & (lane < to + n), v, tiles[tt])
                done += n

    def state_prep(l):
        step = jnp.broadcast_to(ls_v[pl.ds(l, 1), :], (GROUPS, GROUPS))
        diag = lax.broadcasted_iota(jnp.int32, (GROUPS, GROUPS), 0) == lanes_of((GROUPS, GROUPS))
        step = jnp.exp(jnp.sum(jnp.where(diag, step, 0.0), axis=1, keepdims=True))
        lr, li = -dec_v[l], frq_v[l]
        mag, ang = jnp.exp(lr * step), li * step
        are, aim = mag * jnp.cos(ang), mag * jnp.sin(ang)
        den = lr * lr + li * li
        nre = are - 1.0
        zre, zim = (nre * lr + aim * li) / den, (aim * lr - nre * li) / den
        a1 = jnp.concatenate([are, are], axis=1)
        a2 = jnp.concatenate([-aim, aim], axis=1)
        spread = lambda v: jnp.broadcast_to(v[:, None, :], (GROUPS, GS, PS)).reshape(C, PS)
        zre, zim = spread(zre), spread(zim)
        ire, iim = ire_v[l], iim_v[l]
        bmat = jnp.concatenate([zre * ire - zim * iim, zre * iim + zim * ire], axis=1)
        cmat = jnp.concatenate([rre_v[l], -rim_v[l]], axis=1)
        of = lax.broadcasted_iota(jnp.int32, (C, 128), 0) // GS
        for g in range(GROUPS):
            at = pl.ds(g * 128, 128)
            b_hi[l, :, at], b_lo[l, :, at] = parts(jnp.where(of == g, bmat, 0.0))
            c_hi[l, :, at], c_lo[l, :, at] = parts(jnp.where(of == g, cmat, 0.0))
            h = jnp.concatenate([st_v[0, l, pl.ds(g, B, stride=GROUPS), :],
                                 st_v[1, l, pl.ds(g, B, stride=GROUPS), :]], axis=1)
            s_v[l, :, at] = a1[g:g + 1] * h + a2[g:g + 1] * pltpu.roll(h, PS, 1)

    def mixer(l, drive, gate, sq):
        sq = jnp.sum(jnp.where((lane128 >= 96) & (lane128 < 98), sq, 0.0), axis=1, keepdims=True)
        inverse = lax.rsqrt(sq * (1.0 / D) + 1e-06)
        drive, gate = drive * inverse, gate * inverse
        uh, ul = parts(drive)
        bh, bl = b_hi[l], b_lo[l]
        h = s_v[l] + (dot(uh, bh) + (dot(uh, bl) + dot(ul, bh)))
        hh, hl = parts(h)
        ch, cl = c_hi[l], c_lo[l]
        out = dot_t(hh, ch) + (dot_t(hh, cl) + dot_t(hl, ch))
        out = out + skip_v[pl.ds(l, 1), :] * drive
        s_v[l] = h
        gelu = 0.5 * out * (1.0 + jnp.tanh(0.7978845608028654 * (out + 0.044715 * (out * out * out))))
        return (gelu * (1.0 / (1.0 + jnp.exp(-gate)))).astype(BF)

    def store_states(l):
        for g in range(GROUPS):
            h = s_v[l, :, pl.ds(g * 128, 128)]
            next_re[l, pl.ds(g, B, stride=GROUPS), :] = h[:, :PS]
            next_im[l, pl.ds(g, B, stride=GROUPS), :] = pltpu.roll(h, PS, 1)[:, :PS]

    def to_blocks(l, total):
        tiles = [total[:, t * 128:(t + 1) * 128] for t in range(TILES)]
        for k in range(NZ):
            t, s = divmod(k * F, 128)
            v = pltpu.roll(tiles[t], 128 - s, 1) if s else tiles[t]
            if s + F > 128:
                w = pltpu.roll(tiles[t + 1], 128 - s, 1)
                v = jnp.where(lane128 < 128 - s, v, w)
            zsend[l, k] = v.astype(BF)

    def z_reduce(l, meanwhile):
        with scope("zsc_start"):
            scatter(f"zs{l}", zsend.at[l], zrecv.at[l], "z", NZ, z)
        meanwhile()
        with scope("zsc_wait"):
            arrived(f"zs{l}", zrecv.at[l])
        with scope("z_sum"):
            total = zsend[l, z].astype(F32)
            for h in range(NZ - 1):
                total = total + zrecv[l, h].astype(F32)
            return jnp.where(lane128 < F, res_v[...] + total, 0.0).astype(BF)

    with scope("publish"):
        res_v[...] = jnp.zeros((B, 128), F32)
        res_v[:, :F] = tok_v[...].astype(F32)
        publish(0, res_v[...])
    with scope("barrier"):
        pl.semaphore_wait(barrier, len(greet))

    with scope("zag_start"):
        gather("zg0", zbuf.at[0], "z", NZ, z)
    with scope("loads"):
        for cp in wloads0:
            cp.wait()
    with scope("x_start0"):
        ring0("r_in", 0, x, right)
        ring0("l_gate", 1, x, left)
        ring0("r_gate", 1, x, right)
        ring0("l_in", 0, x, left)
        ring0("m_in", 0, x, mate)
        ring0("m_gate", 1, x, mate)
    with scope("e0_start"):
        for cp in wloads1:
            cp.wait()
        exchange1(0)
    with scope("prep0"):
        state_prep(0)
    with scope("zag_wait"):
        arrived("zg0", zbuf.at[0, pl.ds(0, NZ - 1)])
    with scope("compact"):
        def write0(t, v):
            ybuf[y, :, t * 128:(t + 1) * 128] = v
        compact(0, write0)
    with scope("yag_start"):
        gather("yg0", ybuf, "y", NY, y)
        exchange1(1)
    with scope("x01_0"):
        ring0_wait("r_in")
        ring0_wait("l_gate")
        ring0("rr_in", 0, x_of(NX - 1), right)
        ring0("ll_gate", 1, x_of(1), left)
        ring0("ml_in", 0, x_of(NX - 1), mate)
        ring0("mr_gate", 1, x_of(1), mate)
    with scope("prep1"):
        state_prep(1)
        rload.wait()
        relayout_out()
        oload.wait()

        @pl.when(has_b)
        def _():
            own_b(0).wait()
            own_b(1).wait()
    with scope("x23_0"):
        ring0_wait("r_gate")
        ring0_wait("l_in")
        ring0("ml_gate", 1, x_of(NX - 1), mate)
        ring0("mr_in", 0, x_of(1), mate)
    with scope("yag_wait"):
        arrived("yg0", ybuf.at[pl.ds(0, NY - 1)])
    with scope("x45_0"):
        ring0_wait("rr_in")
        ring0_wait("ll_gate")
    with scope("x_start1"):
        ring0("m2_in", 0, x_of(2), mate)
        ring0("m2_gate", 1, x_of(2), mate)
        exchange1_wait(0)
        ring1("R_in", 0, x, right)
        ring1("L_in", 0, x, left)
        ring1("M_in", 0, x, mate)
    with scope("c_wait"):
        for k in ("m_in", "m_gate", "ml_in", "mr_gate", "ml_gate", "mr_in", "m2_in", "m2_gate"):
            ring0_wait(k)
    with scope("mixer"):
        drive = jnp.zeros((B, C), F32)
        gate = jnp.zeros((B, C), F32)
        sq = jnp.zeros((B, 128), F32)
        for k in range(NY):
            a = ybuf[k]
            drive = drive + dot(a[:, :K], win_v[0, k])
            gate = gate + dot(a[:, :K], wg_v[0, k])
            sq = sq + a[:, KP - 128:].astype(F32)
        gated = mixer(0, drive, gate, sq)
    with scope("project"):
        part_v[...] = dot(gated, wout_v[...])
        for yy in range(NY):
            tiles = [jnp.zeros((B, 128), F32) for _ in range(TILES)]
            by_y(lambda st: part_v[:, st * 128:(st + 1) * 128], yy, tiles, lane128)
            for t in range(TILES):
                rsend[yy, :, t * 128:(t + 1) * 128] = tiles[t].astype(BF)
    with scope("ysc_start"):
        scatter("ys0", rsend, rrecv, "y", NY, y)
    with scope("store_states"):
        store_states(0)
    with scope("e1_wait"):
        exchange1_wait(1)
        ring1("R_gate", 1, x, right)
        ring1("L_gate", 1, x, left)
        ring1("M_gate", 1, x, mate)
    with scope("x_in1"):
        ring1_wait("R_in")
        ring1("RR_in", 0, x_of(NX - 1), right)
        ring1("Ml_in", 0, x_of(NX - 1), mate)
        ring1_wait("L_in")
        ring1("Mr_in", 0, x_of(1), mate)
    with scope("ysc_wait"):
        arrived("ys0", rrecv)
    with scope("y_sum"):
        total = rsend[y].astype(F32)
        for h in range(NY - 1):
            total = total + rrecv[h].astype(F32)
        to_blocks(0, total)

    def out_exchange():
        copies = []
        for h in far_first(NY):
            to = lax.rem(y + h, NY)
            copies.append((wsend_v.at[to], wo_v.at[y, d16], {"y": to}))
        group("oy", copies, wo_v.at[pl.ds(0, NY - 1), pl.ds(0, 16)])

    def after_z0():
        with scope("o_start"):
            out_exchange()
        with scope("x_gate1"):
            ring1_wait("L_gate")
            ring1("LL_gate", 1, x_of(1), left)
            ring1("Mr_gate", 1, x_of(1), mate)
            ring1_wait("R_gate")
            ring1("Ml_gate", 1, x_of(NX - 1), mate)

    new = z_reduce(0, after_z0)
    res_v[...] = new.astype(F32)
    publish(1, new.astype(F32))

    with scope("zag_start"):
        gather("zg1", zbuf.at[1], "z", NZ, z)
    with scope("x2_1"):
        ring1_wait("RR_in")
        ring1("M2_in", 0, x_of(2), mate)
        ring1_wait("LL_gate")
        ring1("M2_gate", 1, x_of(2), mate)

    def out_ring(key, h, peer, half):
        r = wo_v.at[half, wo_rows(h, c)]
        group(key, [(r, r, peer)], r)

    every, low, high = pl.ds(0, NY), pl.ds(0, NY // 2), pl.ds(NY // 2, NY // 2)
    with scope("o_x"):
        arrived("oy", wo_v.at[pl.ds(0, NY - 1), pl.ds(0, 16)])
        out_ring("or", 0, right, every)
        out_ring("ol", 0, left, every)
        out_ring("om", 0, mate, every)
    with scope("zag_wait"):
        arrived("zg1", zbuf.at[1, pl.ds(0, NZ - 1)])
    with scope("compact"):
        def write1(t, v):
            xl_v[:, t * 128:(t + 1) * 128] = v
        compact(1, write1)
    with scope("c_wait1"):
        for k in ("M_in", "M_gate", "Ml_in", "Mr_in", "Ml_gate", "Mr_gate", "M2_in", "M2_gate"):
            mate1_wait(k)
    with scope("partial"):
        a = xl_v[...]
        for k in range(NY):
            psend[k, :, 0:128] = dot(a[:, :K], win_v[1, k]).astype(BF)
            psend[k, :, 128:256] = dot(a[:, :K], wg_v[1, k]).astype(BF)
            psend[k, :, 256:384] = a[:, KP - 128:]
    with scope("ysc_start"):
        scatter("ys1", psend, precv, "y", NY, y)
    with scope("o_x2"):
        arrived("or", wo_v.at[every, pl.ds(0, 16)])
        out_ring("orr", NX - 1, right, low)
        out_ring("oml", NX - 1, mate, every)
        arrived("ol", wo_v.at[every, pl.ds(0, 16)])
        out_ring("oll", 1, left, high)
        out_ring("omr", 1, mate, every)
    with scope("ysc_wait"):
        arrived("ys1", precv)
    with scope("mixer"):
        total = psend[y].astype(F32)
        for h in range(NY - 1):
            total = total + precv[h].astype(F32)
        gated = mixer(1, total[:, :128], total[:, 128:256], total[:, 256:])
        gbuf[y] = gated
    with scope("gag_start"):
        gather("gg", gbuf, "y", NY, y)
    with scope("store_states"):
        store_states(1)
    with scope("o_x3"):
        arrived("orr", wo_v.at[low, pl.ds(0, 16)])
        arrived("oll", wo_v.at[high, pl.ds(0, 16)])
        out_ring("om2", 2, mate, every)
    with scope("gag_wait"):
        arrived("gg", gbuf.at[pl.ds(0, NY - 1)])
    with scope("o_wait"):
        for k in ("om", "oml", "omr", "om2"):
            arrived(k, wo_v.at[every, pl.ds(0, 16)])
    with scope("project"):
        total = dot(gbuf[0], wo_v[0])
        for k in range(1, NY):
            total = total + dot(gbuf[k], wo_v[k])
        to_blocks(1, total)
    new = z_reduce(1, lambda: None)
    mixed[...] = new[:, :F]
    with scope("finish"):
        for key, size in unsent:
            remote(size, size, key, mate).wait_send()
        for key, size, when in part_sent:
            pl.when(when)(lambda key=key, size=size: remote(size, size, key, mate).wait_send())
    assert len(names) <= SEMS, len(names)


def write_out(a, b, c, to_a, to_b, to_c, sems):
    copies = [pltpu.make_async_copy(v, o, sems.at[i])
              for i, (v, o) in enumerate(((b, to_b), (c, to_c), (a, to_a)))]
    for cp in copies:
        cp.start()
    for cp in copies:
        cp.wait()


def on_device(tokens, gains, w_in, w_gate, w_out, decay, freq, log_step, in_re, in_im, ro_re, ro_im,
              skip, st_re, st_im):
    blocks = lambda w: w.reshape(LAYERS, NZ, F, C)
    flat = lambda s: s.reshape(LAYERS, B * GROUPS, PS)
    cols = lambda m: m.transpose(0, 1, 3, 2).reshape(LAYERS, C, PS)
    wide = lambda m: m.reshape(LAYERS, C, PS)
    args = (tokens, gains, blocks(w_in), blocks(w_gate), w_out, decay, freq, log_step, cols(in_re),
            cols(in_im), wide(ro_re), wide(ro_im), skip, flat(st_re), flat(st_im))
    any_ = pl.BlockSpec(memory_space=pl.ANY)
    V = pltpu.VMEM
    sem = pltpu.SemaphoreType.DMA
    L = LAYERS
    scratch = [
        V((B, F), BF), V((L, D), F32),
        V((L, NY, K, C), BF), V((L, NY, K, C), BF), V((2, NZ, F, C), BF), V((C, D), BF),
        V((16, D), BF), V((NY, 16, KP), BF), V((NY, C, KP), BF),
        V((L, GROUPS, PS), F32), V((L, GROUPS, PS), F32), V((L, GROUPS), F32),
        V((L, C, PS), F32), V((L, C, PS), F32), V((L, C, PS), F32), V((L, C, PS), F32), V((L, C), F32),
        V((2, L, B * GROUPS, PS), F32), V((L, B, GROUPS * 128), F32),
        V((L, C, GROUPS * 128), BF), V((L, C, GROUPS * 128), BF),
        V((L, C, GROUPS * 128), BF), V((L, C, GROUPS * 128), BF),
        V((B, 128), F32), V((L, NZ, B, 128), BF), V((NY, B, KP), BF), V((B, KP), BF), V((B, D), F32),
        V((NY, B, KP), BF), V((NY - 1, B, KP), BF),
        V((NY, B, 384), BF), V((NY - 1, B, 384), BF), V((NY, B, C), BF),
        V((L, NZ, B, 128), BF), V((L, NZ - 1, B, 128), BF),
        sem((12,)), sem((12,)), sem((SEMS,)), sem((SEMS,)),
    ]
    shapes = (((B, F), BF), ((L, B * GROUPS, PS), F32), ((L, B * GROUPS, PS), F32))
    vmem = pl.BlockSpec(memory_space=pltpu.VMEM)
    held = pl.pallas_call(
        body,
        name="decode",
        out_shape=tuple(V(*sh) for sh in shapes),
        in_specs=[any_] * len(args),
        out_specs=(vmem,) * 3,
        scratch_shapes=scratch,
        compiler_params=pltpu.CompilerParams(collective_id=0, has_side_effects=True,
                                             vmem_limit_bytes=56 * 2**20),
    )(*args)
    mixed, nre, nim = pl.pallas_call(
        write_out,
        name="write_out",
        out_shape=tuple(jax.ShapeDtypeStruct(*sh) for sh in shapes),
        in_specs=[vmem] * 3,
        out_specs=(any_,) * 3,
        scratch_shapes=[sem((3,))],
    )(*(pltpu.with_memory_space_constraint(v, pltpu.VMEM) for v in held))
    shape = (L, B, GROUPS, PS)
    return mixed, nre.reshape(shape), nim.reshape(shape)


def solution(mesh):
    torus = Mesh(mesh.devices.reshape(NZ, NY, NX, 2), ("z", "y", "x", "c"))
    tp, dp = ("z", "y"), ("x", "c")
    return jax.shard_map(
        on_device,
        mesh=torus,
        in_specs=(
            P(dp, tp), P(), P(None, dp, tp), P(None, dp, tp), P(None, tp, None), P(None, tp, None),
            P(None, tp, None), P(None, tp), P(None, tp, None, None), P(None, tp, None, None),
            P(None, tp, None, None), P(None, tp, None, None), P(None, tp),
            P(None, dp, tp, None), P(None, dp, tp, None),
        ),
        out_specs=(P(dp, tp), P(None, dp, tp, None), P(None, dp, tp, None)),
        check_vma=False,
    )
```

time: 102 us -> 86 us (0.84)
  Pallas kernels: 96.6 us -> 84.7 us
  local copies, waits for them, and re-layouts: 4.52 us -> 0 us
    pallas_call x1 -> x2, Pallas kernels: 96.6 us -> 84.7 us  [the longest x1 83.9 us: on_device(): pl.pallas_call(body, name='decode', out_shape=tuple((V(*sh) for sh in sha...]
    unnamed x3 -> x0, local copies, waits for them, and re-layouts: 4.52 us -> none
where the time goes in v2:
time: 86 us; the launch traced here: 85.3 us
  Pallas kernels  84.7 us (98%)
    pallas_call x1, Pallas kernels, on_device(): pl.pallas_call(body, name='decode', out_shape=tuple((V(*sh) for sh in sha...  83.9 us

profile of v2, /device:TPU:1, one launch (start us, length us, event | category | flops | bytes accessed | tf_op | source)
XLA Modules:
  0.0 85.3 jit_solution(1738664543232800770)
XLA Ops:
  0.6 83.9 %decode.1 = (bf16[24,88]{1,0:T(8,128)(2,1)S(1)}, f32[2,192,64]{2,1,0:T(8,128)S(1)}, f32[2,192,64]{2,1,0:T(8,128)S(1)}) custom-call(bf16[24,88]{1,0:T(8,128)(2,1)} %tokens.1, f32[2,8448]{1,0:T(2,128)} %gains.1, bf16[2,12,88,128]{3,2,1,0:T(8,128)(2,1)} %bitcast.14, bf16[2,12,88,128]{3,2,1,0:T(8,128)(2,1)} %bitcast.15, bf16[2,128,8448]{2,1,0:T(8,128)(2,1)} %w_out.1, ...), custom_call_target="tpu_custom_call" | custom-call | tf_op jit(solution)/shard_map/decode/pallas_call | solution.py:597
  84.6 0.8 write_out.1

commit v3 on v2

--- a/solution.py
+++ b/solution.py
@@ -17,7 +17,9 @@
 K = NZ * F
 KP = 1152
 TILES = KP // 128
-SEMS = 80
+SEMS = 76
+RA, RB = 16, 8
+TZ = 6
 BF = jnp.bfloat16
 F32 = jnp.float32
 
@@ -47,11 +49,12 @@
     tokens, gains, w_in, w_gate, w_out, decay, freq, log_step, in_re, in_im, ro_re, ro_im, skip,
     st_re, st_im,
     mixed, next_re, next_im,
-    tok_v, gain_v, win_v, wg_v, stage_v, wout_v, wrow_v, wsend_v, wo_v,
+    tok_v, gain_v, w_v, stage_v, wout_v, wrow_v, wsend_v, wo_v,
     dec_v, frq_v, ls_v, ire_v, iim_v, rre_v, rim_v, skip_v,
     st_v, s_v, b_hi, b_lo, c_hi, c_lo,
-    res_v, zbuf, ybuf, xl_v, part_v, rsend, rrecv, psend, precv, gbuf, zsend, zrecv,
-    load_sem, wload_sem, ssem, rsem,
+    res_v, zga, ygb, zgb, zbuf, ybuf, acc_v, part_v, rsend, rrecv, psend, precv, gbuf, zsend, zrecv,
+    zsa, zra, zsb, zrb, ysb, yrb,
+    load_sem, wload_sem, ssem, rsem, ready,
 ):
     z, y = lax.axis_index("z"), lax.axis_index("y")
     x, c = lax.axis_index("x"), lax.axis_index("c")
@@ -64,7 +67,8 @@
     right, left, mate = along("x", 1), along("x", NX - 1), along("c", 1)
 
     barrier = pltpu.get_barrier_semaphore()
-    greet = [("z", h) for h in far_first(NZ)] + [("y", h) for h in far_first(NY)]
+    greet = [("z", h) for h in (3, NZ - 3, 2, NZ - 2, 1, NZ - 1)]
+    greet += [("y", h) for h in (2, NY - 2, 1, NY - 1)]
     greet += [("x", 1), ("x", NX - 1), ("c", 1)]
     for ax, h in greet:
         pl.semaphore_signal(barrier, inc=1, device_id=along(ax, h), device_id_type=MESH)
@@ -81,7 +85,7 @@
     def rows(zz):
         return pl.ds(pl.multiple_of(zz * F, 8), F)
 
-    mats = (win_v, wg_v)
+    cols = (pl.ds(0, C), pl.ds(C, C))
     d16 = pl.ds(pl.multiple_of((2 * x + c) * 16, 16), 16)
     za, zb = 3 * x + 2 * c, 3 * x + 1
     has_b = (y // 4) == c
@@ -93,20 +97,20 @@
 
     wloads0 = []
     for m, src in enumerate((w_in, w_gate)):
-        wloads0.append(load(src.at[0, pl.ds(4 * c, 8)], mats[m].at[0, :, rows(za)], 2 * m))
+        wloads0.append(load(src.at[0, pl.ds(4 * c, 8)], w_v.at[0, :, rows(za), cols[m]], 2 * m))
         wloads0.append(load(src.at[0, pl.ds(8 - 8 * c, 4)],
-                            mats[m].at[0, pl.ds(4 * c, 4), rows(zb)], 2 * m + 1))
+                            w_v.at[0, pl.ds(4 * c, 4), rows(zb), cols[m]], 2 * m + 1))
     oload = load(w_out.at[0], wout_v, 4)
     wloads1 = []
     for m, src in enumerate((w_in, w_gate)):
         wloads1.append(load(src.at[1], stage_v.at[m], 5 + m))
-        wloads1.append(load(src.at[1, 4 * c + y], mats[m].at[1, y, rows(za)], 7 + m))
+        wloads1.append(load(src.at[1, 4 * c + y], w_v.at[1, y, rows(za), cols[m]], 7 + m))
     rload = load(w_out.at[1, d16], wrow_v, 9)
 
     def own_b(m):
         src = (w_in, w_gate)[m]
         return pltpu.make_async_copy(
-            src.at[1, 8 - 8 * c + lax.rem(y, 4)], mats[m].at[1, y, rows(zb)], wload_sem.at[10 + m])
+            src.at[1, 8 - 8 * c + lax.rem(y, 4)], w_v.at[1, y, rows(zb), cols[m]], wload_sem.at[10 + m])
 
     @pl.when(has_b)
     def _():
@@ -120,7 +124,7 @@
 
     def remote(src, dst, key, peer):
         k = sem_of(key)
-        return pltpu.make_async_remote_copy(src_ref=src, dst_ref=dst, send_sem=ssem.at[k],
+        return pltpu.make_async_remote_copy(src_ref=src, dst_ref=dst, send_sem=ssem.at[0],
                                             recv_sem=rsem.at[k], device_id=peer, device_id_type=MESH)
 
     unsent = []
@@ -152,12 +156,14 @@
         hi, lo = parts(jnp.sum(xv * xv, axis=1, keepdims=True))
         out = jnp.where(lane128 < F, scaled, 0.0)
         out = jnp.where(lane128 == F, hi.astype(F32), out)
-        out = jnp.where(lane128 == F + 1, lo.astype(F32), out)
-        zbuf[l, z] = out.astype(BF)
-
-    def gather(key, buf, ax, n, me):
-        group(key, [(buf.at[me], buf.at[me], along(ax, h)) for h in far_first(n)],
-              buf.at[pl.ds(0, n - 1)])
+        return jnp.where(lane128 == F + 1, lo.astype(F32), out).astype(BF)
+
+    def gather(key, buf, ax, n, me, hs, apart=False):
+        for h in hs:
+            group(f"{key}_{h}" if apart else key, [(buf.at[me], buf.at[me], along(ax, h))], buf.at[0])
+
+    def gathered(key, buf, n):
+        arrived(key, buf.at[pl.ds(0, n - 1)])
 
     def scatter(key, src, dst, ax, n, me):
         copies = []
@@ -166,89 +172,94 @@
             copies.append((src.at[to], dst.at[h - 1], {ax: to}))
         group(key, copies, dst)
 
-    def compact(l, write):
-        tiles = [jnp.zeros((B, 128), F32) for _ in range(TILES)]
-        total = jnp.zeros((B, 128), F32)
-        for k in range(NZ):
-            v = zbuf[l, k].astype(F32)
+    def compact(buf, n, tiles_n, write):
+        shape = (buf.shape[1], 128)
+        lane = lanes_of(shape)
+        tiles = [jnp.zeros(shape, F32) for _ in range(tiles_n)]
+        total = jnp.zeros(shape, F32)
+        for k in range(n):
+            v = buf[k].astype(F32)
             total = total + v
             t, s = divmod(k * F, 128)
             r = pltpu.roll(v, s, 1) if s else v
-            tiles[t] = jnp.where((lane128 >= s) & (lane128 < s + F), r, tiles[t])
+            tiles[t] = jnp.where((lane >= s) & (lane < s + F), r, tiles[t])
             if s + F > 128:
-                tiles[t + 1] = jnp.where(lane128 < s + F - 128, r, tiles[t + 1])
-        sq = jnp.sum(jnp.where((lane128 >= F) & (lane128 < F + 2), total, 0.0), axis=1, keepdims=True)
+                tiles[t + 1] = jnp.where(lane < s + F - 128, r, tiles[t + 1])
+        sq = jnp.sum(jnp.where((lane >= F) & (lane < F + 2), total, 0.0), axis=1, keepdims=True)
         hi, lo = parts(sq)
-        last = tiles[TILES - 1]
-        last = jnp.where(lane128 == 96, hi.astype(F32), last)
-        tiles[TILES - 1] = jnp.where(lane128 == 97, lo.astype(F32), last)
-        for t in range(TILES):
+        last = jnp.where(lane == 96, hi.astype(F32), tiles[tiles_n - 1])
+        tiles[tiles_n - 1] = jnp.where(lane == 97, lo.astype(F32), last)
+        for t in range(tiles_n):
             write(t, tiles[t].astype(BF))
 
-    def ring0(key, m, owner_x, peer):
-        w = mats[m]
-        a = w.at[0, :, rows(3 * owner_x + 2 * c)]
-        b = w.at[0, pl.ds(4 * c, 4), rows(3 * owner_x + 1)]
-        group(key, [(a, a, peer), (b, b, peer)], w.at[0, 0, pl.ds(0, K)])
-
-    def ring0_wait(key):
-        arrived(key, win_v.at[0, 0, pl.ds(0, K)])
+    def ring0(key, m, owner_x, peer, which=2):
+        a = w_v.at[0, :, rows(3 * owner_x + 2 * c), cols[m]]
+        b = w_v.at[0, pl.ds(4 * c, 4), rows(3 * owner_x + 1), cols[m]]
+        if which == 2:
+            group(key, [(a, a, peer), (b, b, peer)], w_v.at[0, 0, pl.ds(0, K), cols[0]])
+        else:
+            r = (a, b)[which]
+            group(key, [(r, r, peer)], r)
+
+    def ring0_wait(key, which=2):
+        size = w_v.at[0, 0, pl.ds(0, K), cols[0]]
+        if which < 2:
+            size = w_v.at[0, pl.ds(0, (8, 4)[which]), pl.ds(0, F), cols[0]]
+        arrived(key, size)
 
     def ring1(key, m, owner_x, peer):
-        w = mats[m]
-        a = w.at[1, :, rows(3 * owner_x + 2 * c)]
-        group(key + "a", [(a, a, peer)], a)
-        b = w.at[1, :, rows(3 * owner_x + 1)]
+        a = w_v.at[1, :, rows(3 * owner_x + 2 * c), cols[m]]
+        group(key, [(a, a, peer)], a)
+        b = w_v.at[1, :, rows(3 * owner_x + 1), cols[m]]
 
         @pl.when(has_b)
         def _():
-            remote(b, b, key + "b", peer).start()
-
-        part_sent.append((key + "b", b, has_b))
+            remote(b, b, key, peer).start()
+
+        part_sent.append((key, b, has_b))
 
     part_sent = []
-    blocks8 = win_v.at[1, :, pl.ds(0, F)]
+    no_b = jnp.logical_not(has_b)
+
+    def arrived_either(key, whole):
+        for when, n in ((whole, 2 * F), (jnp.logical_not(whole), F)):
+            @pl.when(when)
+            def _():
+                arrived(key, w_v.at[1, :, pl.ds(0, n), cols[0]])
 
     def ring1_wait(key):
-        arrived(key + "a", blocks8)
-
-        @pl.when(has_b)
-        def _():
-            arrived(key + "b", blocks8)
+        arrived_either(key, has_b)
 
     def mate1_wait(key):
-        arrived(key + "a", blocks8)
-
-        @pl.when(jnp.logical_not(has_b))
-        def _():
-            arrived(key + "b", blocks8)
+        arrived_either(key, no_b)
+
+    def blocks(n):
+        return w_v.at[1, pl.ds(0, n), pl.ds(0, F), cols[0]]
 
     def exchange1(m):
-        key, w = f"e{m}", mats[m]
-        dst = w.at[1, y, rows(za)]
+        key = f"e{m}"
+        dst = w_v.at[1, y, rows(za), cols[m]]
         copies = []
         for h in far_first(NY):
             to = lax.rem(y + h, NY)
             copies.append((stage_v.at[m, 4 * c + to], dst, {"y": to}))
-        group(key + "a", copies, w.at[1, pl.ds(0, NY - 1), pl.ds(0, F)])
-        dst_b = w.at[1, y, rows(zb)]
+        group(key, copies, blocks(NY - 1))
+        dst_b = w_v.at[1, y, rows(zb), cols[m]]
         for k in range(4):
             to = 4 * c + k
 
             @pl.when(to != y)
             def _():
-                remote(stage_v.at[m, 8 - 8 * c + k], dst_b, key + "b", {"y": to}).start()
-
-        part_sent.append((key + "b", w.at[1, pl.ds(0, 3), pl.ds(0, F)], has_b))
-        part_sent.append((key + "b", w.at[1, pl.ds(0, 4), pl.ds(0, F)], jnp.logical_not(has_b)))
+                remote(stage_v.at[m, 8 - 8 * c + k], dst_b, key, {"y": to}).start()
+
+        part_sent.append((key, blocks(3), has_b))
+        part_sent.append((key, blocks(4), no_b))
 
     def exchange1_wait(m):
-        key, w = f"e{m}", mats[m]
-        arrived(key + "a", w.at[1, pl.ds(0, NY - 1), pl.ds(0, F)])
-
-        @pl.when(has_b)
-        def _():
-            arrived(key + "b", w.at[1, pl.ds(0, NY - 1), pl.ds(0, F)])
+        for when, n in ((has_b, 2 * F), (no_b, F)):
+            @pl.when(when)
+            def _():
+                arrived(f"e{m}", w_v.at[1, pl.ds(0, NY - 1), pl.ds(0, n), cols[0]])
 
     x_of = lambda h: lax.rem(x + h, NX)
     names_of = ("in", "gate")
@@ -266,8 +277,11 @@
         wo_v[y, d16] = wsend_v[y]
 
     def by_y(tile_of, yy, tiles, lane):
+        runs(tiles, lane, lambda k: ((k * NY + yy) * F, tile_of))
+
+    def runs(tiles, lane, source):
         for k in range(NZ):
-            lo, done = (k * NY + yy) * F, 0
+            (lo, tile_of), done = source(k), 0
             while done < F:
                 st, so = divmod(lo + done, 128)
                 tt, to = divmod(k * F + done, 128)
@@ -324,37 +338,31 @@
             next_re[l, pl.ds(g, B, stride=GROUPS), :] = h[:, :PS]
             next_im[l, pl.ds(g, B, stride=GROUPS), :] = pltpu.roll(h, PS, 1)[:, :PS]
 
-    def to_blocks(l, total):
+    def to_blocks(into, total):
         tiles = [total[:, t * 128:(t + 1) * 128] for t in range(TILES)]
+        lane = lanes_of(tiles[0].shape)
         for k in range(NZ):
             t, s = divmod(k * F, 128)
             v = pltpu.roll(tiles[t], 128 - s, 1) if s else tiles[t]
             if s + F > 128:
                 w = pltpu.roll(tiles[t + 1], 128 - s, 1)
-                v = jnp.where(lane128 < 128 - s, v, w)
-            zsend[l, k] = v.astype(BF)
-
-    def z_reduce(l, meanwhile):
-        with scope("zsc_start"):
-            scatter(f"zs{l}", zsend.at[l], zrecv.at[l], "z", NZ, z)
-        meanwhile()
-        with scope("zsc_wait"):
-            arrived(f"zs{l}", zrecv.at[l])
-        with scope("z_sum"):
-            total = zsend[l, z].astype(F32)
-            for h in range(NZ - 1):
-                total = total + zrecv[l, h].astype(F32)
-            return jnp.where(lane128 < F, res_v[...] + total, 0.0).astype(BF)
+                v = jnp.where(lane < 128 - s, v, w)
+            into[k] = v.astype(BF)
 
     with scope("publish"):
         res_v[...] = jnp.zeros((B, 128), F32)
         res_v[:, :F] = tok_v[...].astype(F32)
-        publish(0, res_v[...])
+        out = publish(0, res_v[...])
+        zga[z] = out[:RA]
+        ygb[y] = out[RA:]
     with scope("barrier"):
         pl.semaphore_wait(barrier, len(greet))
-
-    with scope("zag_start"):
-        gather("zg0", zbuf.at[0], "z", NZ, z)
+        for ax, h, k in (("z", 3, 0), ("z", NZ - 3, 0), ("y", 2, 1), ("y", NY - 2, 1)):
+            pl.semaphore_signal(ready.at[k], inc=1, device_id=along(ax, h), device_id_type=MESH)
+
+    near_z, near_y = (3, NZ - 3, 2, NZ - 2, 1, NZ - 1), (2, NY - 2, 1, NY - 1)
+    far_z = [h for h in far_first(NZ) if h not in near_z]
+    far_y = [h for h in far_first(NY) if h not in near_y]
     with scope("loads"):
         for cp in wloads0:
             cp.wait()
@@ -365,26 +373,43 @@
         ring0("l_in", 0, x, left)
         ring0("m_in", 0, x, mate)
         ring0("m_gate", 1, x, mate)
-    with scope("e0_start"):
+    with scope("ag_start"):
+        gather("zga", zga, "z", NZ, z, near_z)
+        gather("ygb", ygb, "y", NY, y, near_y)
         for cp in wloads1:
             cp.wait()
+        pl.semaphore_wait(ready.at[1], 2)
+        gather("ygb", ygb, "y", NY, y, far_y)
+        pl.semaphore_wait(ready.at[0], 2)
+        gather("zga", zga, "z", NZ, z, far_z)
+    with scope("e0_start"):
         exchange1(0)
     with scope("prep0"):
         state_prep(0)
-    with scope("zag_wait"):
-        arrived("zg0", zbuf.at[0, pl.ds(0, NZ - 1)])
+    with scope("ygb_wait"):
+        gathered("ygb", ygb, NY)
+    with scope("compact_b"):
+        def write_b(t, v):
+            zgb[z, :, t * 128:(t + 1) * 128] = v
+        compact(ygb, NY, TZ, write_b)
+    with scope("zgb_start"):
+        gather("zgb", zgb, "z", NZ, z, far_first(NZ))
+    with scope("zga_wait"):
+        gathered("zga", zga, NZ)
     with scope("compact"):
-        def write0(t, v):
-            ybuf[y, :, t * 128:(t + 1) * 128] = v
-        compact(0, write0)
-    with scope("yag_start"):
-        gather("yg0", ybuf, "y", NY, y)
+        def write_a(t, v):
+            ybuf[y, :RA, t * 128:(t + 1) * 128] = v
+        compact(zga, NZ, TILES, write_a)
+    with scope("yga_start"):
+        a_rows = ybuf.at[:, pl.ds(0, RA)]
+        gather("yga", a_rows, "y", NY, y, far_first(NY))
         exchange1(1)
     with scope("x01_0"):
         ring0_wait("r_in")
         ring0_wait("l_gate")
-        ring0("rr_in", 0, x_of(NX - 1), right)
-        ring0("ll_gate", 1, x_of(1), left)
+        for k in range(2):
+            ring0(f"rr_in{k}", 0, x_of(NX - 1), right, k)
+            ring0(f"ll_gate{k}", 1, x_of(1), left, k)
         ring0("ml_in", 0, x_of(NX - 1), mate)
         ring0("mr_gate", 1, x_of(1), mate)
     with scope("prep1"):
@@ -402,36 +427,67 @@
         ring0_wait("l_in")
         ring0("ml_gate", 1, x_of(NX - 1), mate)
         ring0("mr_in", 0, x_of(1), mate)
-    with scope("yag_wait"):
-        arrived("yg0", ybuf.at[pl.ds(0, NY - 1)])
+    with scope("zgb_wait"):
+        gathered("zgb", zgb, NZ)
+    with scope("regroup_b"):
+        lane8 = lanes_of((RB, 128))
+        sq_b = jnp.zeros((RB, 128), F32)
+        for k in range(NZ):
+            sq_b = sq_b + zgb[k, :, (TZ - 1) * 128:].astype(F32)
+        for yy in range(NY):
+            tiles = [jnp.zeros((RB, 128), F32) for _ in range(TILES)]
+            runs(tiles, lane8, lambda k: (yy * F, lambda st: zgb[k, :, st * 128:(st + 1) * 128].astype(F32)))
+            for t in range(TILES):
+                ybuf[yy, RA:, t * 128:(t + 1) * 128] = tiles[t].astype(BF)
+    with scope("yga_wait"):
+        gathered("yga", a_rows, NY)
     with scope("x45_0"):
-        ring0_wait("rr_in")
-        ring0_wait("ll_gate")
+        for k in range(2):
+            ring0_wait(f"rr_in{k}", k)
+            ring0(f"m2_in{k}", 0, x_of(2), mate, k)
+            ring0_wait(f"ll_gate{k}", k)
+            ring0(f"m2_gate{k}", 1, x_of(2), mate, k)
     with scope("x_start1"):
-        ring0("m2_in", 0, x_of(2), mate)
-        ring0("m2_gate", 1, x_of(2), mate)
         exchange1_wait(0)
         ring1("R_in", 0, x, right)
         ring1("L_in", 0, x, left)
         ring1("M_in", 0, x, mate)
     with scope("c_wait"):
-        for k in ("m_in", "m_gate", "ml_in", "mr_gate", "ml_gate", "mr_in", "m2_in", "m2_gate"):
+        for k in ("m_in", "m_gate", "ml_in", "mr_gate", "ml_gate", "mr_in"):
             ring0_wait(k)
+        for k in range(2):
+            ring0_wait(f"m2_in{k}", k)
+            ring0_wait(f"m2_gate{k}", k)
     with scope("mixer"):
         drive = jnp.zeros((B, C), F32)
         gate = jnp.zeros((B, C), F32)
-        sq = jnp.zeros((B, 128), F32)
+        sq_a = jnp.zeros((RA, 128), F32)
         for k in range(NY):
             a = ybuf[k]
-            drive = drive + dot(a[:, :K], win_v[0, k])
-            gate = gate + dot(a[:, :K], wg_v[0, k])
-            sq = sq + a[:, KP - 128:].astype(F32)
+            drive = drive + dot(a[:, :K], w_v[0, k, :, :C])
+            gate = gate + dot(a[:, :K], w_v[0, k, :, C:])
+            sq_a = sq_a + a[:RA, KP - 128:].astype(F32)
+        sq = jnp.concatenate([sq_a, sq_b], axis=0)
         gated = mixer(0, drive, gate, sq)
     with scope("project"):
         part_v[...] = dot(gated, wout_v[...])
+        for k in range(NZ):
+            for t in range(TZ):
+                st, so = divmod(k * NY * F + t * 128, 128)
+                v = part_v[RA:, st * 128:(st + 1) * 128]
+                if so:
+                    v = pltpu.roll(v, 64, 1)
+                    if t < TZ - 1:
+                        w = part_v[RA:, (st + 1) * 128:(st + 2) * 128]
+                        v = jnp.where(lane8 < 64, v, pltpu.roll(w, 64, 1))
+                zsb[k, :, t * 128:(t + 1) * 128] = v.astype(BF)
+    with scope("zb_start"):
+        scatter("zb", zsb, zrb, "z", NZ, z)
+    with scope("project_a"):
+        lane16 = lanes_of((RA, 128))
         for yy in range(NY):
-            tiles = [jnp.zeros((B, 128), F32) for _ in range(TILES)]
-            by_y(lambda st: part_v[:, st * 128:(st + 1) * 128], yy, tiles, lane128)
+            tiles = [jnp.zeros((RA, 128), F32) for _ in range(TILES)]
+            by_y(lambda st: part_v[:RA, st * 128:(st + 1) * 128], yy, tiles, lane16)
             for t in range(TILES):
                 rsend[yy, :, t * 128:(t + 1) * 128] = tiles[t].astype(BF)
     with scope("ysc_start"):
@@ -449,13 +505,29 @@
         ring1("Ml_in", 0, x_of(NX - 1), mate)
         ring1_wait("L_in")
         ring1("Mr_in", 0, x_of(1), mate)
+    with scope("zb_wait"):
+        arrived("zb", zrb)
+    with scope("zb_sum"):
+        total = zsb[z].astype(F32)
+        for h in range(NZ - 1):
+            total = total + zrb[h].astype(F32)
+        for yy in range(NY):
+            t, so = divmod(yy * F, 128)
+            v = total[:, t * 128:(t + 1) * 128]
+            v = pltpu.roll(v, 128 - so, 1) if so else v
+            if so + F > 128:
+                w = pltpu.roll(total[:, (t + 1) * 128:(t + 2) * 128], 128 - so, 1)
+                v = jnp.where(lane8 < 128 - so, v, w)
+            ysb[yy] = v.astype(BF)
+    with scope("yb_start"):
+        scatter("yb", ysb, yrb, "y", NY, y)
     with scope("ysc_wait"):
         arrived("ys0", rrecv)
     with scope("y_sum"):
         total = rsend[y].astype(F32)
         for h in range(NY - 1):
             total = total + rrecv[h].astype(F32)
-        to_blocks(0, total)
+        to_blocks(zsa, total)
 
     def out_exchange():
         copies = []
@@ -464,22 +536,34 @@
             copies.append((wsend_v.at[to], wo_v.at[y, d16], {"y": to}))
         group("oy", copies, wo_v.at[pl.ds(0, NY - 1), pl.ds(0, 16)])
 
-    def after_z0():
-        with scope("o_start"):
-            out_exchange()
-        with scope("x_gate1"):
-            ring1_wait("L_gate")
-            ring1("LL_gate", 1, x_of(1), left)
-            ring1("Mr_gate", 1, x_of(1), mate)
-            ring1_wait("R_gate")
-            ring1("Ml_gate", 1, x_of(NX - 1), mate)
-
-    new = z_reduce(0, after_z0)
+    with scope("zsc_start"):
+        scatter("zs0", zsa, zra, "z", NZ, z)
+    with scope("o_start"):
+        out_exchange()
+    with scope("x_gate1"):
+        ring1_wait("L_gate")
+        ring1("LL_gate", 1, x_of(1), left)
+        ring1("Mr_gate", 1, x_of(1), mate)
+        ring1_wait("R_gate")
+        ring1("Ml_gate", 1, x_of(NX - 1), mate)
+    with scope("yb_wait"):
+        arrived("yb", yrb)
+    with scope("zsc_wait"):
+        arrived("zs0", zra)
+    with scope("z_sum"):
+        total = zsa[z].astype(F32)
+        for h in range(NZ - 1):
+            total = total + zra[h].astype(F32)
+        low_rows = ysb[y].astype(F32)
+        for h in range(NY - 1):
+            low_rows = low_rows + yrb[h].astype(F32)
+        total = jnp.concatenate([total, low_rows], axis=0)
+        new = jnp.where(lane128 < F, res_v[...] + total, 0.0).astype(BF)
     res_v[...] = new.astype(F32)
-    publish(1, new.astype(F32))
+    zbuf[z] = publish(1, new.astype(F32))
 
     with scope("zag_start"):
-        gather("zg1", zbuf.at[1], "z", NZ, z)
+        gather("zg1", zbuf, "z", NZ, z, far_first(NZ), True)
     with scope("x2_1"):
         ring1_wait("RR_in")
         ring1("M2_in", 0, x_of(2), mate)
@@ -493,33 +577,40 @@
     every, low, high = pl.ds(0, NY), pl.ds(0, NY // 2), pl.ds(NY // 2, NY // 2)
     with scope("o_x"):
         arrived("oy", wo_v.at[pl.ds(0, NY - 1), pl.ds(0, 16)])
-        out_ring("or", 0, right, every)
-        out_ring("ol", 0, left, every)
+        out_ring("or_l", 0, right, low)
+        out_ring("ol_h", 0, left, high)
+        out_ring("or_h", 0, right, high)
+        out_ring("ol_l", 0, left, low)
         out_ring("om", 0, mate, every)
-    with scope("zag_wait"):
-        arrived("zg1", zbuf.at[1, pl.ds(0, NZ - 1)])
-    with scope("compact"):
-        def write1(t, v):
-            xl_v[:, t * 128:(t + 1) * 128] = v
-        compact(1, write1)
     with scope("c_wait1"):
         for k in ("M_in", "M_gate", "Ml_in", "Mr_in", "Ml_gate", "Mr_gate", "M2_in", "M2_gate"):
             mate1_wait(k)
     with scope("partial"):
-        a = xl_v[...]
-        for k in range(NY):
-            psend[k, :, 0:128] = dot(a[:, :K], win_v[1, k]).astype(BF)
-            psend[k, :, 128:256] = dot(a[:, :K], wg_v[1, k]).astype(BF)
-            psend[k, :, 256:384] = a[:, KP - 128:]
+        sq = jnp.zeros((B, 128), F32)
+        for i, h in enumerate([0] + far_first(NZ)[::-1]):
+            if h:
+                arrived(f"zg1_{h}", zbuf.at[0])
+            k = lax.rem(z + NZ - h, NZ)
+            a = zbuf[k]
+            sq = sq + a.astype(F32)
+            for yy in range(NY):
+                v = dot(a[:, :F], w_v[1, yy, rows(k), :])
+                acc_v[yy] = acc_v[yy] + v if i else v
+        sq = jnp.where((lane128 >= F) & (lane128 < F + 2), sq, 0.0)
+        hi, lo = parts(jnp.sum(sq, axis=1, keepdims=True))
+        sq = jnp.where(lane128 == 96, hi.astype(F32), jnp.where(lane128 == 97, lo.astype(F32), 0.0))
+        for yy in range(NY):
+            psend[yy, :, :2 * C] = acc_v[yy].astype(BF)
+            psend[yy, :, 2 * C:] = sq.astype(BF)
     with scope("ysc_start"):
         scatter("ys1", psend, precv, "y", NY, y)
     with scope("o_x2"):
-        arrived("or", wo_v.at[every, pl.ds(0, 16)])
+        arrived("or_l", wo_v.at[low, pl.ds(0, 16)])
         out_ring("orr", NX - 1, right, low)
-        out_ring("oml", NX - 1, mate, every)
-        arrived("ol", wo_v.at[every, pl.ds(0, 16)])
+        out_ring("oml_l", NX - 1, mate, low)
+        arrived("ol_h", wo_v.at[high, pl.ds(0, 16)])
         out_ring("oll", 1, left, high)
-        out_ring("omr", 1, mate, every)
+        out_ring("omr_h", 1, mate, high)
     with scope("ysc_wait"):
         arrived("ys1", precv)
     with scope("mixer"):
@@ -529,31 +620,45 @@
         gated = mixer(1, total[:, :128], total[:, 128:256], total[:, 256:])
         gbuf[y] = gated
     with scope("gag_start"):
-        gather("gg", gbuf, "y", NY, y)
+        gather("gg", gbuf, "y", NY, y, far_first(NY), True)
     with scope("store_states"):
         store_states(1)
     with scope("o_x3"):
+        arrived("or_h", wo_v.at[high, pl.ds(0, 16)])
+        out_ring("oml_h", NX - 1, mate, high)
+        arrived("ol_l", wo_v.at[low, pl.ds(0, 16)])
+        out_ring("omr_l", 1, mate, low)
         arrived("orr", wo_v.at[low, pl.ds(0, 16)])
+        out_ring("om2_l", 2, mate, low)
         arrived("oll", wo_v.at[high, pl.ds(0, 16)])
-        out_ring("om2", 2, mate, every)
-    with scope("gag_wait"):
-        arrived("gg", gbuf.at[pl.ds(0, NY - 1)])
+        out_ring("om2_h", 2, mate, high)
     with scope("o_wait"):
-        for k in ("om", "oml", "omr", "om2"):
-            arrived(k, wo_v.at[every, pl.ds(0, 16)])
+        arrived("om", wo_v.at[every, pl.ds(0, 16)])
+        for k in ("oml", "omr", "om2"):
+            arrived(k + "_l", wo_v.at[low, pl.ds(0, 16)])
+            arrived(k + "_h", wo_v.at[high, pl.ds(0, 16)])
     with scope("project"):
-        total = dot(gbuf[0], wo_v[0])
-        for k in range(1, NY):
+        total = dot(gated, wo_v[y])
+        for h in far_first(NY)[::-1]:
+            arrived(f"gg_{h}", gbuf.at[0])
+            k = lax.rem(y + NY - h, NY)
             total = total + dot(gbuf[k], wo_v[k])
-        to_blocks(1, total)
-    new = z_reduce(1, lambda: None)
-    mixed[...] = new[:, :F]
+        to_blocks(zsend, total)
+    with scope("zsc_start"):
+        scatter("zs1", zsend, zrecv, "z", NZ, z)
+    with scope("zsc_wait"):
+        arrived("zs1", zrecv)
+    with scope("z_sum"):
+        total = zsend[z].astype(F32)
+        for h in range(NZ - 1):
+            total = total + zrecv[h].astype(F32)
+        mixed[...] = (res_v[...] + total).astype(BF)[:, :F]
     with scope("finish"):
         for key, size in unsent:
             remote(size, size, key, mate).wait_send()
         for key, size, when in part_sent:
             pl.when(when)(lambda key=key, size=size: remote(size, size, key, mate).wait_send())
-    assert len(names) <= SEMS, len(names)
+    assert len(names) == SEMS, len(names)
 
 
 def write_out(a, b, c, to_a, to_b, to_c, sems):
@@ -579,18 +684,23 @@
     L = LAYERS
     scratch = [
         V((B, F), BF), V((L, D), F32),
-        V((L, NY, K, C), BF), V((L, NY, K, C), BF), V((2, NZ, F, C), BF), V((C, D), BF),
+        V((L, NY, K, 2 * C), BF), V((2, NZ, F, C), BF), V((C, D), BF),
         V((16, D), BF), V((NY, 16, KP), BF), V((NY, C, KP), BF),
         V((L, GROUPS, PS), F32), V((L, GROUPS, PS), F32), V((L, GROUPS), F32),
         V((L, C, PS), F32), V((L, C, PS), F32), V((L, C, PS), F32), V((L, C, PS), F32), V((L, C), F32),
         V((2, L, B * GROUPS, PS), F32), V((L, B, GROUPS * 128), F32),
         V((L, C, GROUPS * 128), BF), V((L, C, GROUPS * 128), BF),
         V((L, C, GROUPS * 128), BF), V((L, C, GROUPS * 128), BF),
-        V((B, 128), F32), V((L, NZ, B, 128), BF), V((NY, B, KP), BF), V((B, KP), BF), V((B, D), F32),
-        V((NY, B, KP), BF), V((NY - 1, B, KP), BF),
+        V((B, 128), F32), V((NZ, RA, 128), BF), V((NY, RB, 128), BF), V((NZ, RB, TZ * 128), BF),
+        V((NZ, B, 128), BF), V((NY, B, KP), BF), V((NY, B, 2 * C), F32), V((B, D), F32),
+        V((NY, RA, KP), BF), V((NY - 1, RA, KP), BF),
         V((NY, B, 384), BF), V((NY - 1, B, 384), BF), V((NY, B, C), BF),
-        V((L, NZ, B, 128), BF), V((L, NZ - 1, B, 128), BF),
-        sem((12,)), sem((12,)), sem((SEMS,)), sem((SEMS,)),
+        V((NZ, B, 128), BF), V((NZ - 1, B, 128), BF),
+        V((NZ, RA, 128), BF), V((NZ - 1, RA, 128), BF),
+        V((NZ, RB, TZ * 128), BF), V((NZ - 1, RB, TZ * 128), BF),
+        V((NY, RB, 128), BF), V((NY - 1, RB, 128), BF),
+        sem((12,)), sem((12,)), sem((1,)), sem((SEMS,)),
+        pltpu.SemaphoreType.REGULAR((2,)),
     ]
     shapes = (((B, F), BF), ((L, B * GROUPS, PS), F32), ((L, B * GROUPS, PS), F32))
     vmem = pl.BlockSpec(memory_space=pltpu.VMEM)

time: 86 us -> 78.9 us (0.917)
  Pallas kernels: 84.7 us -> 77.8 us
    pallas_call x1, Pallas kernels: 83.9 us -> 77.1 us  [on_device(): pl.pallas_call(body, name='decode', out_shape=tuple((V(*sh) for sh in sha...]
where the time goes in v3:
time: 78.9 us; the launch traced here: 78.5 us
  Pallas kernels  77.8 us (99%)
    pallas_call x1, Pallas kernels, on_device(): pl.pallas_call(body, name='decode', out_shape=tuple((V(*sh) for sh in sha...  77.1 us

profile of v3, /device:TPU:1, one launch (start us, length us, event | category | flops | bytes accessed | tf_op | source)
XLA Modules:
  0.0 78.5 jit_solution(3317373906004858317)
XLA Ops:
  0.6 77.1 %decode.1 = (bf16[24,88]{1,0:T(8,128)(2,1)S(1)}, f32[2,192,64]{2,1,0:T(8,128)S(1)}, f32[2,192,64]{2,1,0:T(8,128)S(1)}) custom-call(bf16[24,88]{1,0:T(8,128)(2,1)} %tokens.1, f32[2,8448]{1,0:T(2,128)} %gains.1, bf16[2,12,88,128]{3,2,1,0:T(8,128)(2,1)} %bitcast.14, bf16[2,12,88,128]{3,2,1,0:T(8,128)(2,1)} %bitcast.15, bf16[2,128,8448]{2,1,0:T(8,128)(2,1)} %w_out.1, ...), custom_call_target="tpu_custom_call" | custom-call | tf_op jit(solution)/shard_map/decode/pallas_call | solution.py:707
  77.7 0.8 write_out.1
